TPU v7x, 256 devices: a whole 4x4x8 slice. The times are simulated.
256 devices in a mesh: sp: 32 (over z, y), tp: 8 (over x, core).
Axes of the slice: x: 4, y: 4, z: 8, core: 2. Of those that a mesh axis runs over, the one named last changes fastest.
Arguments:
- queries: bfloat16 [32768, 1024], P('sp', 'tp'), may hold values from -6 to 6
- cell_key_rows: bfloat16 [32768, 1024], P('sp', 'tp'), may hold values from -6 to 6
- cell_value_rows: bfloat16 [32768, 2048], P('sp', 'tp'), may hold values from -6 to 6
- output_gate_logits: bfloat16 [32768, 2048], P('sp', 'tp'), may hold values from -6 to 6
- input_gate_logits: bfloat16 [8, 32768], P('tp', 'sp'), may hold values from -4 to 216
- forget_gate_logits: bfloat16 [8, 32768], P('tp', 'sp'), may hold values from 0.5 to 14
- forget_extra_term: float32 [8, 32768], P('tp', 'sp'), may hold values from -1.4 to 0
- residual: bfloat16 [32768, 2048], P('sp', 'tp'), may hold values from -13 to 13
- head_norm_gain: bfloat16 [2048], P('tp'), may hold values from 0.099609375 to 1.8984375
- cell_output_weight: bfloat16 [2048, 2048], P('tp'), may hold values from -0.25 to 0.25
- feedforward_norm_gain: bfloat16 [2048], replicated, may hold values from 0.099609375 to 1.8984375
- gate_projection_weight: bfloat16 [2048, 5632], P('sp', 'tp'), may hold values from -0.125 to 0.125
- up_projection_weight: bfloat16 [2048, 5632], P('sp', 'tp'), may hold values from -0.125 to 0.125
- down_projection_weight: bfloat16 [5632, 2048], P('tp', 'sp'), may hold values from -0.15625 to 0.15625
Outputs:
- mixed: bfloat16 [32768, 2048], P('sp', 'tp')
All inputs are finite; a program needn't handle non-finite values.
Results may differ from a plain program's by a relative error of at most 0.017.
Values may be sent and summed in bfloat16 or wider, within the bound.
A program may use at most 64 MiB of HBM per device.

v0:
```python
import jax
import jax.numpy as jnp
from jax import lax
from jax.sharding import Mesh
from jax.sharding import PartitionSpec as P

SP = ("sp_0", "sp_1")


PRECISE = lax.Precision.HIGHEST
LOWEST_LOG = -1e30
EPSILON = 1e-06


def gather_turned(arrays, axis, dims):
    turned = [jnp.moveaxis(a, dim, 0) for a, dim in zip(arrays, dims)]
    both = jnp.concatenate([t.reshape(len(t), -1) for t in turned], axis=1)
    filled, at, outs = (lax.all_gather(both, axis, axis=0, tiled=True), 0, [])
    for t, dim in zip(turned, dims):
        section = filled[:, at : at + t[0].size].reshape(-1, *t.shape[1:])
        outs.append(jnp.moveaxis(section, 0, dim))
        at += t[0].size
    return tuple(outs)


def filled_with(array, identity):
    return jax.tree.map(
        lambda a, e: jnp.broadcast_to(jnp.asarray(e, a.dtype), a.shape), array, identity
    )


def collected_together(array, axis):
    leaves = jax.tree.leaves(array)
    turns = sorted(range(len(leaves)), key=lambda k: -leaves[k].size)
    width = (1, *leaves[turns[0]].shape)[-1]
    lines = [
        jnp.pad(leaves[k].reshape(-1), (0, -leaves[k].size % width)).reshape(-1, width)
        for k in turns
    ]
    both, at, found = (lax.all_gather(jnp.concatenate(lines), axis), 0, {})
    for k, line in zip(turns, lines):
        section = both[:, at : at + len(line)].reshape(len(both), -1)
        found[k] = section[:, : leaves[k].size].reshape(-1, *leaves[k].shape)
        at += len(line)
    numbers = iter(range(len(leaves)))
    return jax.tree.map(lambda _: found[next(numbers)], array)


def entering(array, axes, combine, identity):
    before = start = filled_with(array, identity)
    total = array
    for axis in reversed(axes):
        length, index = (lax.axis_size(axis), lax.axis_index(axis))
        pieces = collected_together(total, axis)
        inside, total = (start, start)
        for k in range(length):
            passed = k < index
            total = combine(total, jax.tree.map(lambda part: part[k], pieces))
            inside = jax.tree.map(lambda new, old: jnp.where(passed, new, old), total, inside)
        before = combine(inside, before)
    return before


def cut_along(array, dim, length):
    before, after = (array.shape[:dim], array.shape[dim + 1 :])
    return jnp.moveaxis(array.reshape(*before, length, -1, *after), dim, 0)


def sum_at_owner(array, axis, dim):
    tiles = cut_along(array, dim, lax.axis_size(axis))
    arrived = lax.all_to_all(tiles, axis, split_axis=0, concat_axis=0, tiled=True)
    return arrived.astype(jnp.float32).sum(axis=0)


def to_blocks(array, block_count, block_size):
    shaped = array.reshape((array.shape[0], block_count, block_size) + array.shape[2:])
    return jnp.moveaxis(shaped, 1, 0)


def from_blocks(array):
    moved = jnp.moveaxis(array, 0, 1)
    return moved.reshape((moved.shape[0], moved.shape[1] * moved.shape[2]) + moved.shape[3:])


def memory_blocks(
    query_raw, key_raw, value_heads, in_gates, forget_log_value, block_size, query_scale
):
    head_count, length, key_width = query_raw.shape
    value_width = value_heads.shape[2]
    block_count = length // block_size
    causal = jnp.tril(jnp.ones((block_size, block_size), bool))

    def advance(carried, pieces):
        memory_state, top_log, offset = carried
        query_block, key_block, value_block, gate_block, forget_block = pieces
        running = jnp.cumsum(forget_block, axis=-1)
        log_weight = jnp.where(
            causal, running[:, :, None] - running[:, None, :] + gate_block[:, None, :], -jnp.inf
        )
        log_start = running + top_log[:, None]
        row_max = jnp.maximum(jnp.max(log_weight, axis=-1), log_start)
        scores = jnp.einsum(
            "htd,hsd->hts", query_block, key_block, preferred_element_type=jnp.float32
        )
        scores = scores * query_scale * jnp.exp(log_weight - row_max[:, :, None])
        query_wide = query_block.astype(jnp.float32) * query_scale
        earlier = jnp.einsum("htd,hde->hte", query_wide, memory_state, precision=PRECISE)
        numerator = jnp.exp(log_start - row_max)[:, :, None] * earlier
        numerator = numerator + jnp.einsum("hts,hse->hte", scores, value_block, precision=PRECISE)
        last_cum = running[:, -1]
        log_end = last_cum[:, None] - running + gate_block
        new_top = jnp.maximum(last_cum + top_log, jnp.max(log_end, axis=-1))
        scaled = key_block.astype(jnp.float32) * jnp.exp(log_end - new_top[:, None])[:, :, None]
        memory_state = jnp.exp(last_cum + top_log - new_top)[:, None, None] * memory_state
        memory_state = memory_state + jnp.einsum(
            "hsd,hse->hde", scaled, value_block, precision=PRECISE
        )
        return (
            (memory_state, new_top, offset + last_cum),
            (numerator, row_max, offset[:, None] + running),
        )

    initial = (
        jnp.zeros((head_count, key_width, value_width), jnp.float32),
        jnp.full((head_count,), LOWEST_LOG, jnp.float32),
        jnp.zeros((head_count,), jnp.float32),
    )
    pieces = tuple(
        (
            to_blocks(array, block_count, block_size)
            for array in (query_raw, key_raw, value_heads, in_gates, forget_log_value)
        )
    )
    ending, outputs = lax.scan(advance, initial, pieces)
    return (tuple((from_blocks(output) for output in outputs)), ending)


def join_states(earlier, later):
    state_early, top_early, total_early = earlier
    state_late, top_late, total_late = later
    moved_top = top_early + total_late
    new_top = jnp.maximum(moved_top, top_late)
    joined = jnp.exp(moved_top - new_top)[:, None, None] * state_early
    joined = joined + jnp.exp(top_late - new_top)[:, None, None] * state_late
    return (joined, new_top, total_early + total_late)


def heads_first(array, head_count):
    token_rows = array.shape[0]
    width = array.shape[1] // head_count
    return jnp.transpose(array.reshape(token_rows, head_count, width), (1, 0, 2))


def local(
    queries,
    cell_key_rows,
    cell_value_rows,
    output_gate_logits,
    input_gate_logits,
    forget_gate_logits,
    forget_extra_term,
    residual,
    head_norm_gain,
    cell_output_weight,
    feedforward_norm_gain,
    gate_projection_weight,
    up_projection_weight,
    down_projection_weight,
):
    whole_gate, whole_up, whole_down = gather_turned(
        (gate_projection_weight, up_projection_weight, down_projection_weight), SP, (0, 0, 1)
    )
    token_rows = queries.shape[0]
    head_count = input_gate_logits.shape[0]
    key_width = queries.shape[1] // head_count
    value_width = cell_value_rows.shape[1] // head_count
    query_scale = key_width ** (-0.5)
    query_raw = heads_first(queries, head_count)
    key_raw = heads_first(cell_key_rows, head_count)
    value_heads = heads_first(cell_value_rows, head_count).astype(jnp.float32)
    forget_log_value = (
        jax.nn.log_sigmoid(forget_gate_logits.astype(jnp.float32)) + forget_extra_term
    )
    results, ending = memory_blocks(
        query_raw,
        key_raw,
        value_heads,
        input_gate_logits.astype(jnp.float32),
        forget_log_value,
        min(token_rows, 512),
        query_scale,
    )
    numerator, local_max, offsets = results
    end_state, end_top, end_total = ending
    identity = (
        jnp.zeros_like(end_state),
        jnp.full_like(end_top, LOWEST_LOG),
        jnp.zeros_like(end_total),
    )
    carried_state, carried_top, _ = entering(
        (end_state, end_top, end_total), SP, join_states, identity
    )
    shifted = offsets + carried_top[:, None]
    row_max = jnp.maximum(local_max, shifted)
    query_heads = query_raw.astype(jnp.float32) * query_scale
    from_before = jnp.einsum("htd,hde->hte", query_heads, carried_state, precision=PRECISE)
    memory = (
        jnp.exp(local_max - row_max)[:, :, None] * numerator
        + jnp.exp(shifted - row_max)[:, :, None] * from_before
    )
    memory = jnp.transpose(memory, (1, 0, 2))
    normal = memory * lax.rsqrt(jnp.mean(memory * memory, axis=-1, keepdims=True) + EPSILON)
    gate_open = jax.nn.sigmoid(
        output_gate_logits.astype(jnp.float32).reshape(token_rows, head_count, value_width)
    )
    gated_heads = (
        normal * head_norm_gain.astype(jnp.float32).reshape(head_count, value_width) * gate_open
    )
    gated_heads = gated_heads.reshape(token_rows, head_count * value_width).astype(jnp.bfloat16)
    partial_value = jnp.dot(
        gated_heads, cell_output_weight, preferred_element_type=jnp.float32
    ).astype(jnp.bfloat16)
    column_count = residual.shape[1]
    column_start = lax.axis_index("tp") * column_count
    placed = lax.dynamic_update_slice(
        jnp.zeros(partial_value.shape, jnp.float32),
        residual.astype(jnp.float32),
        (jnp.int32(0), column_start),
    )
    stream_rows = lax.psum((partial_value.astype(jnp.float32) + placed).astype(jnp.bfloat16), "tp")
    stream_wide = stream_rows.astype(jnp.float32)
    scale = lax.rsqrt(jnp.mean(stream_wide * stream_wide, axis=1, keepdims=True) + EPSILON)
    normed = (stream_wide * scale * feedforward_norm_gain.astype(jnp.float32)).astype(jnp.bfloat16)
    stream = lax.dynamic_slice_in_dim(stream_rows, column_start, column_count, 1)
    gate_value = jnp.dot(normed, whole_gate, preferred_element_type=jnp.float32)
    lifted = jnp.dot(normed, whole_up, preferred_element_type=jnp.float32)
    hidden = (jax.nn.silu(gate_value) * lifted).astype(jnp.bfloat16)
    down_terms = jnp.dot(hidden, whole_down, preferred_element_type=jnp.float32)
    channel_total = sum_at_owner(down_terms.astype(jnp.bfloat16), "tp", 1)
    return (stream.astype(jnp.float32) + 0.5 * channel_total).astype(jnp.bfloat16)


def solution(mesh):
    torus = Mesh(mesh.devices.reshape(8, 4, mesh.shape["tp"]), ("sp_0", "sp_1", "tp"))
    in_specs = (
        P(SP, "tp"),
        P(SP, "tp"),
        P(SP, "tp"),
        P(SP, "tp"),
        P("tp", SP),
        P("tp", SP),
        P("tp", SP),
        P(SP, "tp"),
        P("tp"),
        P("tp", None),
        P(),
        P(SP, "tp"),
        P(SP, "tp"),
        P("tp", SP),
    )
    out_specs = P(SP, "tp")
    return jax.shard_map(local, mesh=torus, in_specs=in_specs, out_specs=out_specs, check_vma=False)
```

profile of v0, /device:TPU:1, one launch (start us, length us, event | category | flops | bytes accessed | tf_op | source)
XLA Modules:
  0.0 314.5 jit_solution(4814695099431460472)
XLA Ops:
  7.4 1.2 convert.4
  8.6 1.3 convert.3
  9.9 1.3 fusion.143
  11.2 28.4 %while.21 = (s32[]{:T(128)}, f32[1,128,256]{2,1,0:T(8,128)S(1)}, f32[1]{0:T(128)}, f32[1]{0:T(128)}, f32[2,1,512,256]{3,2,1,0:T(8,128)}, /*index=5*/f32[2,1,512]...) while((s32[]{:T(128)}, f32[1,128,256]{2,1,0:T(8,128)S(1)}, ...), condition=%wide.region_5.6_spmd.clone, body=%wide.region_0.5_spmd.clone.sunk | while | flops 1278941696 | bytes 6822432 | solution.py:134
  11.2 0.7 constant_dynamic-slice_fusion.4
  11.9 0.3 reduce-window.14
  12.2 0.2 slice_reduce_fusion.2
  12.4 0.2 reduce-window.15
  12.6 0.1 broadcast.368
  12.7 0.6 slice.453
  13.3 1.9 fusion.179
  16.5 0.7 subtract_exponential_fusion.3
  17.2 0.2 fusion.181
  17.5 0.6 add_maximum_fusion.2
  18.0 1.3 fusion.182
  19.4 1.5 convolution_multiply_fusion.4
  20.9 1.8 fusion.183
  22.8 0.7 fusion.180
  23.6 0.6 copy-done.10
  24.1 0.6 copy-done.13
  25.4 0.7 constant_dynamic-slice_fusion.4
  26.1 0.3 reduce-window.14
  26.4 0.2 slice_reduce_fusion.2
  26.6 0.2 reduce-window.15
  26.8 0.1 broadcast.368
  26.9 0.6 slice.453
  27.5 1.9 fusion.179
  30.7 0.7 subtract_exponential_fusion.3
  31.4 0.2 fusion.181
  31.7 0.6 add_maximum_fusion.2
  32.3 1.3 fusion.182
  33.6 1.5 convolution_multiply_fusion.4
  35.1 1.8 fusion.183
  37.0 0.7 fusion.180
  37.8 0.6 copy-done.10
  38.3 0.6 copy-done.13
  39.6 12.8 %all-gather.2 = f32[4,130,256]{2,1,0:T(8,128)S(1)} all-gather(f32[1,130,256]{2,1,0:T(8,128)S(1)} %maximum_bitcast_fusion), channel_id=2, replica_groups=mesh['sp_0'=8,'sp_1'=4,'tp'=8] {'sp_1'}, dimensions={0}, use_global_device_ids=true | all-gather | bytes 665600 | tf_op jit(solution)/shard_map/all_gather | solution.py:40
  52.5 0.6 fusion.152
  55.1 0.6 fusion.151
  64.4 0.1 fusion.156
  64.5 0.7 maximum_bitcast_fusion.1
  66.0 1.6 copy.22
  67.6 1.2 copy.20
  68.9 34.6 %all-gather.9.cloned.1.call-done = f32[8,130,256]{2,1,0:T(8,128)} async-done(((f32[1,130,256]{2,1,0:T(8,128)}), f32[8,130,256]{2,1,0:T(8,128)}) %all-gather.9.cloned.1.call-update) | async-done | bytes 1064976 | tf_op jit(solution)/shard_map/all_gather | solution.py:40
  103.5 0.9 fusion.147
  104.4 0.6 fusion.150
  105.0 0.6 fusion.149
  121.2 2.8 multiply_reduce_fusion
  124.0 1.5 convert_convert_fusion
  125.5 0.2 add_dynamic-update-slice_fusion.1
  125.7 2.6 convert_element_type.100
  128.3 0.2 all-gather.7.cloned.1.call-start
  128.6 0.6 copy-done.5
  129.3 0.8 concatenate.11
  130.2 78.9 %all-reduce.6.cloned.1.call-done = bf16[1024,2048]{1,0:T(8,128)(2,1)} async-done(((bf16[1024,2048]{1,0:T(8,128)(2,1)}), bf16[1024,2048]{1,0:T(8,128)(2,1)}) %all-reduce.6.cloned.1.call-update) | async-done | bytes 4194320 | tf_op jit(solution)/shard_map/psum | solution.py:230
  209.0 3.2 %fusion.36 = f32[1024]{0:T(1024)S(1)} fusion(bf16[1024,2048]{1,0:T(8,128)(2,1)} %all-reduce.6.cloned.1.call-done), kind=kLoop, calls=%fused_computation.54 | loop fusion | flops 6290432 | bytes 4198400 | tf_op jit(solution)/shard_map/reduce_sum | solution.py:232
  212.2 22.1 %all-gather.7.cloned.1.call-done = bf16[2048,2112]{1,0:T(8,128)(2,1)} async-done(((bf16[64,2112]{1,0:T(8,128)(2,1)}), bf16[2048,2112]{1,0:T(8,128)(2,1)}) %all-gather.7.cloned.1.call-update) | async-done | bytes 8650768 | tf_op jit(solution)/shard_map/all_gather | solution.py:18
  234.3 9.0 %fusion.40 = f32[1024,704]{0,1:T(8,128)S(1)} fusion(bf16[2048,2112]{1,0:T(8,128)(2,1)} %all-gather.7.cloned.1.call-done, bf16[1024,2048]{1,0:T(8,128)(2,1)} %all-reduce.6.cloned.1.call-done, f32[2048]{0:T(1024)S(1)} %convert_element_type.103, f32[1024]{0:T(1024)S(1)} %add_rsqrt_fusion), kind=kOutput, calls=%fused_computation.62 | convolution fusion | flops 2961178624 | bytes 10235904 | tf_op jit(solution)/shard_map/dot_general | solution.py:236
  243.3 3.9 %multiply_convert_fusion = bf16[1024,704]{0,1:T(8,128)(2,1)S(1)} fusion(f32[1024,704]{0,1:T(8,128)S(1)} %fusion.40, bf16[2048,2112]{1,0:T(8,128)(2,1)S(1)} %copy-done.15, bf16[1024,2048]{1,0:T(8,128)(2,1)S(1)} %copy-done.1, f32[2048]{0:T(1024)S(1)} %convert_element_type.103, f32[1024]{0:T(1024)S(1)} %add_rsqrt_fusion), kind=kOutput, calls=%fused_computation.66 | convolution fusion | flops 2965504000 | bytes 11677696 | tf_op jit(solution)/shard_map/dot_general | solution.py:235
  247.2 3.8 %convolution_convert_fusion = bf16[1024,2048]{1,0:T(8,128)(2,1)S(1)} fusion(bf16[1024,704]{0,1:T(8,128)(2,1)S(1)} %multiply_convert_fusion, bf16[2048,2112]{1,0:T(8,128)(2,1)S(1)} %copy-done.15), kind=kOutput, calls=%fused_computation.60 | convolution fusion | flops 2954887168 | bytes 8781824 | tf_op jit(solution)/shard_map/dot_general | solution.py:238
  251.0 0.3 copy.33
  251.3 54.1 %all_to_all.5 = bf16[8,1024,256]{2,1,0:T(8,128)(2,1)S(1)} all-to-all(bf16[8,1024,256]{2,1,0:T(8,128)(2,1)S(1)} %bitcast.229), channel_id=1, replica_groups=mesh['sp_0'=8,'sp_1'=4,'tp'=8] {'tp'}, dimensions={0} | all-to-all | bytes 8388608 | tf_op jit(solution)/shard_map/all_to_all | solution.py:71
  305.4 0.6 convert_reduce_fusion
  306.0 1.0 add_convert_fusion
  (69 shorter events, 0.4 us)
Async XLA Ops:
  7.4 116.6 %copy-start = (bf16[256,2048]{1,0:T(8,128)(2,1)S(1)}, bf16[256,2048]{1,0:T(8,128)(2,1)}, u32[]{:S(2)}) copy-start(bf16[256,2048]{1,0:T(8,128)(2,1)} %param.25) | copy-start | bytes 3145732
  7.4 96.1 %all-gather.9.cloned.1.call-start = ((), (), s32[]{:S(2)}) async-start(), calls=%async_computation.3 | async-start | bytes 1253376 | tf_op jit(solution)/shard_map/all_gather | solution.py:40
  11.2 11.6 %copy-start.2 = (bf16[2,1,512,128]{3,2,1,0:T(8,128)(2,1)S(1)}, bf16[2,1,512,128]{3,2,1,0:T(8,128)(2,1)}, u32[]{:S(2)}) copy-start(bf16[2,1,512,128]{3,2,1,0:T(8,128)(2,1)} %get-tuple-element.318) | copy-start | bytes 786436 | tf_op jit(solution)/shard_map/while
  19.4 4.1 %copy-start.9 = (f32[2,1,512]{2,1,0:T(1,128)S(1)}, f32[2,1,512]{2,1,0:T(1,128)}, u32[]{:S(2)}) copy-start(f32[2,1,512]{2,1,0:T(1,128)} %get-tuple-element.300) | copy-start | bytes 12292 | tf_op jit(solution)/shard_map/while
  19.4 4.1 %copy-start.12 = (f32[2,1,512]{2,1,0:T(1,128)S(1)}, f32[2,1,512]{2,1,0:T(1,128)}, u32[]{:S(2)}) copy-start(f32[2,1,512]{2,1,0:T(1,128)} %get-tuple-element.299) | copy-start | bytes 12292 | tf_op jit(solution)/shard_map/while
  23.6 0.6 copy-start.10
  24.1 0.6 copy-start.13
  25.4 11.6 %copy-start.2 = (bf16[2,1,512,128]{3,2,1,0:T(8,128)(2,1)S(1)}, bf16[2,1,512,128]{3,2,1,0:T(8,128)(2,1)}, u32[]{:S(2)}) copy-start(bf16[2,1,512,128]{3,2,1,0:T(8,128)(2,1)} %get-tuple-element.318) | copy-start | bytes 786436 | tf_op jit(solution)/shard_map/while
  33.6 4.1 %copy-start.9 = (f32[2,1,512]{2,1,0:T(1,128)S(1)}, f32[2,1,512]{2,1,0:T(1,128)}, u32[]{:S(2)}) copy-start(f32[2,1,512]{2,1,0:T(1,128)} %get-tuple-element.300) | copy-start | bytes 12292 | tf_op jit(solution)/shard_map/while
  33.6 4.1 %copy-start.12 = (f32[2,1,512]{2,1,0:T(1,128)S(1)}, f32[2,1,512]{2,1,0:T(1,128)}, u32[]{:S(2)}) copy-start(f32[2,1,512]{2,1,0:T(1,128)} %get-tuple-element.299) | copy-start | bytes 12292 | tf_op jit(solution)/shard_map/while
  37.8 0.6 copy-start.10
  38.3 0.6 copy-start.13
  39.6 29.3 %copy-start.16 = (bf16[256]{0:T(256)(128)(2,1)S(1)}, bf16[256]{0:T(256)(128)(2,1)}, u32[]{:S(2)}) copy-start(bf16[256]{0:T(256)(128)(2,1)} %param.24) | copy-start | bytes 1540
  39.6 81.6 %copy-start.11 = (f32[2,1,512]{2,1,0:T(1,128)S(1)}, f32[2,1,512]{2,1,0:T(1,128)}, u32[]{:S(2)}) copy-start(f32[2,1,512]{2,1,0:T(1,128)} %get-tuple-element.78) | copy-start | bytes 12292
  39.6 81.6 %copy-start.14 = (f32[2,1,512]{2,1,0:T(1,128)S(1)}, f32[2,1,512]{2,1,0:T(1,128)}, u32[]{:S(2)}) copy-start(f32[2,1,512]{2,1,0:T(1,128)} %get-tuple-element.77) | copy-start | bytes 12292
  39.6 81.6 %copy-start.3 = (bf16[2,1,512,128]{3,2,1,0:T(8,128)(2,1)S(1)}, bf16[2,1,512,128]{3,2,1,0:T(8,128)(2,1)}, u32[]{:S(2)}) copy-start(bf16[2,1,512,128]{3,2,1,0:T(8,128)(2,1)} %get-tuple-element.330) | copy-start | bytes 786436
  65.1 143.9 %all-reduce.6.cloned.1.call-start = ((), (), s32[]{:S(2)}) async-start(), calls=%async_computation.1 | async-start | bytes 8388608 | tf_op jit(solution)/shard_map/psum | solution.py:230
  124.0 1.5 copy-start.4
  128.3 0.9 copy-start.5
  128.3 0.9 copy-start.6
  128.3 1.0 copy-start.7
  128.3 1.8 copy-start.8
  128.3 106.0 %all-gather.7.cloned.1.call-start = ((), (), s32[]{:S(2)}) async-start(), calls=%async_computation.2 | async-start | bytes 9191424 | tf_op jit(solution)/shard_map/all_gather | solution.py:18
  234.3 9.0 %copy-start.1 = (bf16[1024,2048]{1,0:T(8,128)(2,1)S(1)}, bf16[1024,2048]{1,0:T(8,128)(2,1)}, u32[]{:S(2)}) copy-start(bf16[1024,2048]{1,0:T(8,128)(2,1)} %all-reduce.6.cloned.1.call-done) | copy-start | bytes 12582916
  234.3 9.0 %copy-start.15 = (bf16[2048,2112]{1,0:T(8,128)(2,1)S(1)}, bf16[2048,2112]{1,0:T(8,128)(2,1)}, u32[]{:S(2)}) copy-start(bf16[2048,2112]{1,0:T(8,128)(2,1)} %all-gather.7.cloned.1.call-done) | copy-start | bytes 25952260
Sparse Core Ops, SparseCore 0:
  65.3 38.1 all-gather.8
  128.5 80.5 all-reduce.5
Sparse Core Ops, SparseCore 1:
  131.4 102.9 all-gather.6
where the time goes:
time: 315 us; the launch traced here: 314 us
  waiting for transfers between devices  136 us (43%)
  blocking collectives  67 us (21%)
  between operations  42.2 us (13%)
  matrix products  31.6 us (10%)
  other arithmetic  20.1 us (6%)
  local copies, waits for them, and re-layouts  13.7 us (4%)
  loops' own time  4.06 us (1%)
    psum x1, waiting for transfers between devices, local(): lax.psum((partial_value.astype(jnp.float32) + placed).astype(jnp.bfloat16...  78.9 us
    all_to_all x1, blocking collectives, sum_at_owner(): lax.all_to_all(tiles, axis, split_axis=0, concat_axis=0, tiled=True)  54.1 us
    all_gather x1, waiting for transfers between devices, collected_together(): both, at, found = (lax.all_gather(jnp.concatenate(lines), axis), 0, {})  34.6 us
    all_gather x1, waiting for transfers between devices, gather_turned(): filled, at, outs = (lax.all_gather(both, axis, axis=0, tiled=True), 0, [])  22.1 us
    all_gather x1, blocking collectives, collected_together(): both, at, found = (lax.all_gather(jnp.concatenate(lines), axis), 0, {})  12.8 us
    dot_general x1, matrix products, local(): lifted = jnp.dot(normed, whole_up, preferred_element_type=jnp.float32)  8.98 us
  transfers between devices with their start and end apart: 3, of which 3 were waited for; matrix products, arithmetic and copies ran while one was open for 2% of the time, Pallas kernels for 0%

commit v1 on v0

v1 whole, which is shorter than its diff:
```python
import jax
import jax.numpy as jnp
from jax import lax
from jax.experimental import pallas as pl
from jax.experimental.pallas import tpu as pltpu
from jax.sharding import Mesh
from jax.sharding import PartitionSpec as P

MESH = pl.DeviceIdType.MESH
F32 = jnp.float32
BF16 = jnp.bfloat16
LOWEST_LOG = -1e30
EPSILON = 1e-06
NZ, NY, NX = 8, 4, 4
CHUNKS = 4


class Slots:
    def __init__(self):
        self.used = 0

    def take(self, count=1):
        first = self.used
        self.used += count
        return first


def running_rows(row, combine, identity):
    length = row.shape[1]
    lane = lax.broadcasted_iota(jnp.int32, row.shape, 1)
    step = 1
    while step < length:
        moved = jnp.where(lane >= step, pltpu.roll(row, step, 1), identity)
        row = combine(row, moved)
        step *= 2
    return row


def as_columns(row):
    return jnp.broadcast_to(row, (128, row.shape[1])).T


def wide(tile, copies):
    return jnp.concatenate([tile] * copies, axis=1)


def join(early, late):
    state_early, top_early, total_early = early
    state_late, top_late, total_late = late
    moved = top_early + total_late
    top = jnp.maximum(moved, top_late)
    left = wide(jnp.exp(moved - top)[0:1], 2)
    right = wide(jnp.exp(top_late - top)[0:1], 2)
    return (left * state_early + right * state_late, top, total_early + total_late)


def load_triple(ref, index):
    part = ref[index]
    return (part[0:32], part[32:40, 0:128], part[32:40, 128:256])


def store_triple(ref, index, triple):
    state, top, total = triple
    ref[index, 0:32, :] = state
    ref[index, 32:40, 0:128] = top
    ref[index, 32:40, 128:256] = total


def cell_kernel(
    q_ref, k_ref, v_ref, og_ref, ig_ref, fg_ref, ex_ref, res_ref, hg_ref, wo_ref, ng_ref,
    gu_in, dn_in,
    out_ref,
    gu_all, dn_all, s1_src, s1_buf, s2_src, s2_buf, s3_src, s3_buf, state_ref,
    num_ref, pbuf, prcv, qbuf, rly, rsum, fin, sbuf, nbuf, hbuf,
    ssem, rsem,
):
    z, y, x, c = (lax.axis_index(a) for a in ("z", "y", "x", "c"))
    rows = q_ref.shape[0]
    chunk = rows // CHUNKS
    half = chunk // 2
    other = 1 - c
    x_at = [lax.rem(x + d, NX) for d in range(NX)]
    y_at = [lax.rem(y + d, NY) for d in range(NY)]
    z_at = [lax.rem(z + d, NZ) for d in range(NZ)]
    to_right, to_left, to_mate = {"x": x_at[1]}, {"x": x_at[3]}, {"c": other}
    y_right, y_left = {"y": y_at[1]}, {"y": y_at[3]}
    z_right, z_left = {"z": z_at[1]}, {"z": z_at[7]}
    sends, slots = [], Slots()

    def send(src, dst, number, device):
        copy = pltpu.make_async_remote_copy(
            src_ref=src, dst_ref=dst, send_sem=ssem.at[number], recv_sem=rsem.at[number],
            device_id=device, device_id_type=MESH,
        )
        copy.start()
        sends.append(copy)

    def arrived(dst, number):
        pltpu.make_async_remote_copy(
            src_ref=dst, dst_ref=dst, send_sem=ssem.at[number], recv_sem=rsem.at[number],
            device_id=to_mate, device_id_type=MESH,
        ).wait_recv()

    for j in range(NZ):
        store_triple(
            s2_buf, j,
            (jnp.zeros((32, 256), F32), jnp.full((8, 128), LOWEST_LOG, F32), jnp.zeros((8, 128), F32)),
        )
    gu_all[z * NY + y] = gu_in[...]
    dn_all[z * NY + y] = dn_in[...]

    barrier = pltpu.get_barrier_semaphore()
    partners = [to_right, to_left, to_mate]
    partners += [{"y": y_at[d]} for d in range(1, NY)] + [{"z": z_at[d]} for d in range(1, NZ)]
    for device in partners:
        pl.semaphore_signal(barrier, inc=1, device_id=device, device_id_type=MESH)
    pl.semaphore_wait(barrier, len(partners))

    gz_r, gz_l = slots.take(4), slots.take(4)
    gy_r, gy_l, gy_fr, gy_fl = slots.take(8), slots.take(8), slots.take(8), slots.take(8)
    dy = slots.take(4)
    dz_r, dz_l = slots.take(4), slots.take(4)
    z_order = [0, 7, 1, 6, 2, 5, 3, 4]
    piece = gu_in.shape[0] // 2

    def gu_z_send(step):
        if step == 0:
            at = gu_all.at[z * NY + y]
            send(gu_in, at, gz_r, z_right)
            send(gu_in, at, gz_l, z_left)
        elif step < 3:
            for number, d, device in ((gz_r, NZ - step, z_right), (gz_l, step, z_left)):
                at = gu_all.at[z_at[d] * NY + y]
                send(at, at, number + step, device)
        else:
            at = gu_all.at[z_at[5] * NY + y, pl.ds(0, piece)]
            send(at, at, gz_r + 3, z_right)
            at = gu_all.at[z_at[3] * NY + y, pl.ds(piece, piece)]
            send(at, at, gz_l + 3, z_left)

    def gu_z_wait(step):
        if step < 3:
            arrived(gu_all.at[z_at[7 - step] * NY + y], gz_r + step)
            arrived(gu_all.at[z_at[1 + step] * NY + y], gz_l + step)
        else:
            arrived(gu_all.at[z_at[4] * NY + y, pl.ds(0, piece)], gz_r + 3)
            arrived(gu_all.at[z_at[4] * NY + y, pl.ds(piece, piece)], gz_l + 3)

    def gu_y_send(k):
        at = gu_all.at[z_at[z_order[k]] * NY + y]
        src = gu_in if k == 0 else at
        send(src, at, gy_r + k, y_right)
        send(src, at, gy_l + k, y_left)

    def gu_y_forward(k):
        block = z_at[z_order[k]] * NY
        arrived(gu_all.at[block + y_at[3]], gy_r + k)
        at = gu_all.at[block + y_at[3], pl.ds(0, piece)]
        send(at, at, gy_fr + k, y_right)
        arrived(gu_all.at[block + y_at[1]], gy_l + k)
        at = gu_all.at[block + y_at[1], pl.ds(piece, piece)]
        send(at, at, gy_fl + k, y_left)

    def gu_y_wait(k):
        block = z_at[z_order[k]] * NY
        arrived(gu_all.at[block + y_at[2], pl.ds(0, piece)], gy_fr + k)
        arrived(gu_all.at[block + y_at[2], pl.ds(piece, piece)], gy_fl + k)

    def dn_y_send():
        at = dn_all.at[z * NY + y]
        send(dn_in, at, dy, y_right)
        send(dn_in, at, dy + 1, y_left)

    def dn_y_forward():
        arrived(dn_all.at[z * NY + y_at[3]], dy)
        at = dn_all.at[z * NY + y_at[3], pl.ds(0, piece)]
        send(at, at, dy + 2, y_right)
        arrived(dn_all.at[z * NY + y_at[1]], dy + 1)
        at = dn_all.at[z * NY + y_at[1], pl.ds(piece, piece)]
        send(at, at, dy + 3, y_left)

    def dn_y_wait():
        arrived(dn_all.at[z * NY + y_at[2], pl.ds(0, piece)], dy + 2)
        arrived(dn_all.at[z * NY + y_at[2], pl.ds(piece, piece)], dy + 3)

    def dn_z_send(step):
        if step < 3:
            for number, d, device in ((dz_r, (NZ - step) % NZ, z_right), (dz_l, step, z_left)):
                at = dn_all.at[pl.ds(z_at[d] * NY, NY)]
                send(at, at, number + step, device)
        else:
            at = dn_all.at[pl.ds(z_at[5] * NY, 2)]
            send(at, at, dz_r + 3, z_right)
            at = dn_all.at[pl.ds(z_at[3] * NY + 2, 2)]
            send(at, at, dz_l + 3, z_left)

    def dn_z_wait(step):
        if step < 3:
            arrived(dn_all.at[pl.ds(z_at[7 - step] * NY, NY)], dz_r + step)
            arrived(dn_all.at[pl.ds(z_at[1 + step] * NY, NY)], dz_l + step)
        else:
            arrived(dn_all.at[pl.ds(z_at[4] * NY, 2)], dz_r + 3)
            arrived(dn_all.at[pl.ds(z_at[4] * NY + 2, 2)], dz_l + 3)

    gu_z_send(0)
    dn_y_send()

    logits = fg_ref[...].astype(F32)
    log_forget = jnp.minimum(logits, 0.0) - jnp.log1p(jnp.exp(-jnp.abs(logits))) + ex_ref[...]
    cum = running_rows(log_forget, jnp.add, 0.0)
    lead = ig_ref[...].astype(F32) - cum
    top_run = running_rows(lead, jnp.maximum, -jnp.inf)
    last_cum = cum[:, rows - 1 :]
    last_lead = top_run[:, rows - 1 :]
    weight = as_columns(jnp.exp(lead - last_lead))
    scaled = (k_ref[...].astype(F32) * weight).astype(BF16)
    end_state = lax.dot_general(
        scaled, v_ref[...], (((0,), (0,)), ((), ())), preferred_element_type=F32
    )
    end_top = jnp.broadcast_to(last_cum + last_lead, (8, 128))
    end_total = jnp.broadcast_to(last_cum, (8, 128))
    for p in range(NY):
        store_triple(s1_src, p, (end_state[p * 32 : p * 32 + 32], end_top, end_total))
    s1, s2, s3 = slots.take(NY), slots.take(NZ), slots.take(NY)
    for d in range(1, NY):
        send(s1_src.at[y_at[d]], s1_buf.at[y], s1 + d, {"y": y_at[d]})
    s1_buf[y] = s1_src[y]
    gu_y_send(0)
    gu_z_wait(0)
    gu_z_send(1)
    gu_y_send(1)
    dn_y_forward()

    top_cols = as_columns(top_run)
    step_rows = 256

    def local_rows(i):
        r0 = i * step_rows
        top_tile = top_cols[r0 : r0 + step_rows]
        parts = None
        for j in range(i + 1):
            s0 = j * step_rows
            scores = lax.dot_general(
                q_ref[r0 : r0 + step_rows], k_ref[s0 : s0 + step_rows],
                (((1,), (1,)), ((), ())), preferred_element_type=F32,
            )
            log_weight = lead[:, s0 : s0 + step_rows] - wide(top_tile, step_rows // 128)
            if i == j:
                at_row = lax.broadcasted_iota(jnp.int32, (step_rows, step_rows), 0)
                at_col = lax.broadcasted_iota(jnp.int32, (step_rows, step_rows), 1)
                log_weight = jnp.where(at_col <= at_row, log_weight, -jnp.inf)
            scores = (scores * (128.0**-0.5) * jnp.exp(log_weight)).astype(BF16)
            term = jnp.dot(scores, v_ref[s0 : s0 + step_rows], preferred_element_type=F32)
            parts = term if parts is None else parts + term
        num_ref[r0 : r0 + step_rows, :] = parts

    local_rows(0)
    local_rows(1)

    for d in range(1, NY):
        arrived(s1_buf.at[y_at[NY - d]], s1 + d)
    inside = [load_triple(s1_buf, 0)]
    for j in range(1, NY):
        inside.append(join(inside[-1], load_triple(s1_buf, j)))
    store_triple(s2_src, 0, inside[-1])
    for d in range(1, NZ):

        @pl.when(z + d < NZ)
        def _(d=d):
            pltpu.make_async_remote_copy(
                src_ref=s2_src.at[0], dst_ref=s2_buf.at[z], send_sem=ssem.at[s2 + d],
                recv_sem=rsem.at[s2 + d], device_id={"z": z_at[d]}, device_id_type=MESH,
            ).start()

    local_rows(2)
    local_rows(3)
    gu_z_wait(1)
    gu_z_send(2)
    gu_y_send(2)
    for d in range(1, NZ):

        @pl.when(z - d >= 0)
        def _(d=d):
            arrived(s2_buf.at[z_at[NZ - d]], s2 + d)

    before = load_triple(s2_buf, 0)
    for j in range(1, NZ):
        before = join(before, load_triple(s2_buf, j))
    store_triple(s3_src, 0, before)
    for j in range(1, NY):
        store_triple(s3_src, j, join(before, inside[j - 1]))
    for d in range(1, NY):
        send(s3_src.at[y_at[d]], s3_buf.at[y], s3 + d, {"y": y_at[d]})
    s3_buf[y] = s3_src[y]
    dn_y_wait()
    gu_z_wait(2)
    gu_z_send(3)
    dn_z_send(0)
    for d in range(1, NY):
        arrived(s3_buf.at[y_at[NY - d]], s3 + d)
    for p in range(NY):
        state_ref[p * 32 : p * 32 + 32, :] = s3_buf[p, 0:32, :].astype(BF16)
    carried_top = s3_buf[0, 32:33, 0:128]

    def reduce_slots():
        return [slots.take(7) for _ in range(CHUNKS)]

    sums = (reduce_slots(), reduce_slots())
    gathers = [slots.take(8) for _ in range(CHUNKS)]

    def swap_send(a, i):
        send(pbuf.at[a, i, other], prcv.at[a, i], sums[a][i], to_mate)

    def swap_join(a, i):
        n = sums[a][i]
        arrived(prcv.at[a, i], n)
        for j in range(NX):
            both = pbuf[a, i, c, j].astype(F32) + prcv[a, i, j].astype(F32)
            qbuf[a, i, j] = both.astype(BF16)
        top, low = pl.ds(0, half), pl.ds(half, half)
        send(qbuf.at[a, i, x_at[2], top], rly.at[a, i, 0], n + 1, to_right)
        send(qbuf.at[a, i, x_at[2], low], rly.at[a, i, 1], n + 2, to_left)
        send(qbuf.at[a, i, x_at[1], low], fin.at[a, i, 0, 1], n + 3, to_right)
        send(qbuf.at[a, i, x_at[3], top], fin.at[a, i, 1, 0], n + 4, to_left)

    def relay(a, i):
        n = sums[a][i]
        arrived(rly.at[a, i, 0], n + 1)
        added = rly[a, i, 0].astype(F32) + qbuf[a, i, x_at[1], 0:half].astype(F32)
        rsum[a, i, 0] = added.astype(BF16)
        send(rsum.at[a, i, 0], fin.at[a, i, 0, 0], n + 5, to_right)
        arrived(rly.at[a, i, 1], n + 2)
        added = rly[a, i, 1].astype(F32) + qbuf[a, i, x_at[3], half:].astype(F32)
        rsum[a, i, 1] = added.astype(BF16)
        send(rsum.at[a, i, 1], fin.at[a, i, 1, 1], n + 6, to_left)

    def total(a, i):
        n = sums[a][i]
        arrived(fin.at[a, i, 0, 1], n + 3)
        arrived(fin.at[a, i, 1, 0], n + 4)
        arrived(fin.at[a, i, 0, 0], n + 5)
        arrived(fin.at[a, i, 1, 1], n + 6)
        found = []
        for h in range(2):
            own = qbuf[a, i, x, h * half : h * half + half].astype(F32)
            found.append(own + fin[a, i, 0, h].astype(F32) + fin[a, i, 1, h].astype(F32))
        return jnp.concatenate(found, axis=0)

    def gated_chunk(i):
        r0 = i * chunk
        part = pl.ds(r0, chunk)
        run = top_cols[r0 : r0 + chunk]
        top = jnp.maximum(run, carried_top)
        keep = wide(jnp.exp(run - top), 2)
        enter = wide(jnp.exp(carried_top - top) * (128.0**-0.5), 2)
        earlier = jnp.dot(q_ref[part], state_ref[...], preferred_element_type=F32)
        memory = keep * num_ref[part] + enter * earlier
        mean = jnp.mean(memory * memory, axis=1, keepdims=True)
        opened = jax.nn.sigmoid(og_ref[part].astype(F32))
        gated = memory * lax.rsqrt(mean + EPSILON) * hg_ref[...].astype(F32) * opened
        gated = gated.astype(BF16)
        for b in range(2 * NX):
            term = jnp.dot(
                gated, wo_ref[:, b * 256 : b * 256 + 256], preferred_element_type=F32
            )
            pbuf[0, i, b % 2, b // 2] = term.astype(BF16)
        swap_send(0, i)

    def stream_chunk(i):
        n = gathers[i]
        summed = total(0, i) + res_ref[pl.ds(i * chunk, chunk)].astype(F32)
        sbuf[i, x, c] = summed.astype(BF16)
        at = sbuf.at[i, x, c]
        send(at, at, n, to_right)
        send(at, at, n + 1, to_left)
        send(at, at, n + 2, to_mate)

    def spread_chunk(i):
        n = gathers[i]
        arrived(sbuf.at[i, x_at[3], c], n)
        at = sbuf.at[i, x_at[3], c, pl.ds(0, half)]
        send(at, at, n + 3, to_right)
        at = sbuf.at[i, x_at[3], c]
        send(at, at, n + 5, to_mate)
        arrived(sbuf.at[i, x_at[1], c], n + 1)
        at = sbuf.at[i, x_at[1], c, pl.ds(half, half)]
        send(at, at, n + 4, to_left)
        at = sbuf.at[i, x_at[1], c]
        send(at, at, n + 6, to_mate)

    def far_chunk(i):
        n = gathers[i]
        arrived(sbuf.at[i, x_at[2], c, pl.ds(0, half)], n + 3)
        arrived(sbuf.at[i, x_at[2], c, pl.ds(half, half)], n + 4)
        at = sbuf.at[i, x_at[2], c]
        send(at, at, n + 7, to_mate)

    def normed_chunk(i):
        n = gathers[i]
        for d, number in ((0, n + 2), (3, n + 5), (1, n + 6), (2, n + 7)):
            arrived(sbuf.at[i, x_at[d], other], number)
        square = jnp.zeros((chunk, 256), F32)
        for b in range(2 * NX):
            part = sbuf[i, b // 2, b % 2].astype(F32)
            square = square + part * part
        mean = jnp.sum(square, axis=1, keepdims=True) * (1.0 / (2 * NX * 256))
        scale = lax.rsqrt(mean + EPSILON)
        for b in range(2 * NX):
            cols = slice(b * 256, b * 256 + 256)
            part = sbuf[i, b // 2, b % 2].astype(F32)
            nbuf[i, :, cols] = (part * scale * ng_ref[:, cols].astype(F32)).astype(BF16)

    def pump(tick):
        if tick == 0:
            gu_y_send(3)
            gu_y_send(4)
        elif tick == 1:
            gu_z_wait(3)
            gu_y_send(5)
            gu_y_send(6)
            gu_y_send(7)
        elif tick == 2:
            dn_z_wait(0)
            dn_z_send(1)
            for k in range(2):
                gu_y_forward(k)
        elif tick == 4:
            dn_z_wait(1)
            dn_z_send(2)
            for k in range(2, 4):
                gu_y_forward(k)
        elif tick == 5:
            for k in range(4, 6):
                gu_y_forward(k)
        elif tick == 6:
            dn_z_wait(2)
            dn_z_send(3)
        elif tick == 7:
            gu_y_forward(6)
            gu_y_forward(7)

    for i in range(CHUNKS):
        gated_chunk(i)
    stages = (
        lambda i: swap_join(0, i), lambda i: relay(0, i), stream_chunk,
        spread_chunk, far_chunk, normed_chunk,
    )
    for tick in range(CHUNKS + len(stages) - 1):
        for lag in range(len(stages)):
            if 0 <= tick - lag < CHUNKS:
                stages[lag](tick - lag)
        pump(tick)

    for k in range(8):
        gu_y_wait(k)

    def up_cols(i, col, width):
        weights = gu_all[:, :, col : col + width].reshape(NZ * NY * 64, width)
        return jnp.dot(nbuf[i], weights, preferred_element_type=F32)

    def silu(v):
        return v / (1.0 + jnp.exp(-v))

    for i in range(CHUNKS):
        for col in (0, 256):
            hidden = silu(up_cols(i, col, 256)) * up_cols(i, 768 + col, 256)
            hbuf[i, :, col : col + 256] = hidden.astype(BF16)
        tail = up_cols(i, 512, 256)
        hidden = silu(tail[:, :128]) * up_cols(i, 1280, 128)
        hbuf[i, :, 512:640] = hidden.astype(BF16)
        mixed_tile = tail[:, 128:]
        hidden = silu(mixed_tile) * pltpu.roll(mixed_tile, 64, 1)
        lane = lax.broadcasted_iota(jnp.int32, hidden.shape, 1)
        hbuf[i, :, 640:768] = jnp.where(lane < 64, hidden, 0.0).astype(BF16)

    dn_z_wait(3)

    def down_chunk(i):
        for b in range(2 * NX):
            weights = dn_all[b * 4 : b * 4 + 4].reshape(256, dn_all.shape[2])
            term = lax.dot_general(
                hbuf[i], weights, (((1,), (1,)), ((), ())), preferred_element_type=F32
            )
            pbuf[1, i, b % 2, b // 2] = term.astype(BF16)
        swap_send(1, i)

    def mixed_chunk(i):
        summed = sbuf[i, x, c].astype(F32) + 0.5 * total(1, i)
        out_ref[pl.ds(i * chunk, chunk)] = summed.astype(BF16)

    stages = (down_chunk, lambda i: swap_join(1, i), lambda i: relay(1, i), mixed_chunk)
    for tick in range(CHUNKS + len(stages) - 1):
        for lag in range(len(stages)):
            if 0 <= tick - lag < CHUNKS:
                stages[lag](tick - lag)

    for copy in sends:
        copy.wait_send()
    for d in range(1, NZ):

        @pl.when(z + d < NZ)
        def _(d=d):
            pltpu.make_async_remote_copy(
                src_ref=s2_src.at[0], dst_ref=s2_buf.at[z], send_sem=ssem.at[s2 + d],
                recv_sem=rsem.at[s2 + d], device_id={"z": z_at[d]}, device_id_type=MESH,
            ).wait_send()


SEMAPHORES = 192


def local(
    queries,
    cell_key_rows,
    cell_value_rows,
    output_gate_logits,
    input_gate_logits,
    forget_gate_logits,
    forget_extra_term,
    residual,
    head_norm_gain,
    cell_output_weight,
    feedforward_norm_gain,
    gate_projection_weight,
    up_projection_weight,
    down_projection_weight,
):
    gate, up, down = gate_projection_weight, up_projection_weight, down_projection_weight
    gate_up = jnp.concatenate([gate, up[:, 640:], up[:, :640]], axis=1)
    down_rows = jnp.pad(down.T, ((0, 0), (0, 64)))
    rows = queries.shape[0]
    chunk = rows // CHUNKS
    half = chunk // 2
    vmem = pltpu.VMEM
    scratch = [
        vmem((NZ * NY, 64, 1408), BF16),
        vmem((NZ * NY, 64, 768), BF16),
        vmem((NY, 40, 256), F32),
        vmem((NY, 40, 256), F32),
        vmem((1, 40, 256), F32),
        vmem((NZ, 40, 256), F32),
        vmem((NY, 40, 256), F32),
        vmem((NY, 40, 256), F32),
        vmem((128, 256), BF16),
        vmem((rows, 256), F32),
        vmem((2, CHUNKS, 2, NX, chunk, 256), BF16),
        vmem((2, CHUNKS, NX, chunk, 256), BF16),
        vmem((2, CHUNKS, NX, chunk, 256), BF16),
        vmem((2, CHUNKS, 2, half, 256), BF16),
        vmem((2, CHUNKS, 2, half, 256), BF16),
        vmem((2, CHUNKS, 2, 2, half, 256), BF16),
        vmem((CHUNKS, NX, 2, chunk, 256), BF16),
        vmem((CHUNKS, chunk, 2048), BF16),
        vmem((CHUNKS, chunk, 768), BF16),
        pltpu.SemaphoreType.DMA((SEMAPHORES,)),
        pltpu.SemaphoreType.DMA((SEMAPHORES,)),
    ]
    return pl.pallas_call(
        cell_kernel,
        out_shape=jax.ShapeDtypeStruct(residual.shape, BF16),
        in_specs=[pl.BlockSpec(memory_space=pltpu.VMEM)] * 13,
        out_specs=pl.BlockSpec(memory_space=pltpu.VMEM),
        scratch_shapes=scratch,
        compiler_params=pltpu.CompilerParams(
            collective_id=0, has_side_effects=True, vmem_limit_bytes=62 * 1024 * 1024
        ),
    )(
        queries,
        cell_key_rows,
        cell_value_rows,
        output_gate_logits,
        input_gate_logits,
        forget_gate_logits,
        forget_extra_term,
        residual,
        head_norm_gain.reshape(1, -1),
        cell_output_weight,
        feedforward_norm_gain.reshape(1, -1),
        gate_up,
        down_rows,
    )


def solution(mesh):
    torus = Mesh(mesh.devices.reshape(NZ, NY, NX, 2), ("z", "y", "x", "c"))
    seq, head = ("z", "y"), ("x", "c")
    in_specs = (
        P(seq, head),
        P(seq, head),
        P(seq, head),
        P(seq, head),
        P(head, seq),
        P(head, seq),
        P(head, seq),
        P(seq, head),
        P(head),
        P(head, None),
        P(),
        P(seq, head),
        P(seq, head),
        P(head, seq),
    )
    return jax.shard_map(
        local, mesh=torus, in_specs=in_specs, out_specs=P(seq, head), check_vma=False
    )
```

time: 315 us -> 121 us (0.38)
  waiting for transfers between devices: 136 us -> 0 us
  Pallas kernels: 0 us -> 114 us
  blocking collectives: 67 us -> 0 us
  between operations: 42.2 us -> 0.02 us
  matrix products: 31.6 us -> 0 us
  other arithmetic: 20.1 us -> 0 us
  local copies, waits for them, and re-layouts: 13.7 us -> 6.87 us
  loops' own time: 4.06 us -> 0 us
    pallas_call x0 -> x1, Pallas kernels: none -> 114 us  [local(): pl.pallas_call(cell_kernel, out_shape=jax.ShapeDtypeStruct(residual.shape...]
    psum x1 -> x0, waiting for transfers between devices: 78.9 us -> none  [local(): lax.psum((partial_value.astype(jnp.float32) + placed).astype(jnp.bfloat16...]
    all_gather x2 -> x0, waiting for transfers between devices: 56.7 us -> none  [the longest x1 34.6 us: collected_together(): both, at, found = (lax.all_gather(jnp.concatenate(lines), axis), 0, {})]
    all_to_all x1 -> x0, blocking collectives: 54.1 us -> none  [sum_at_owner(): lax.all_to_all(tiles, axis, split_axis=0, concat_axis=0, tiled=True)]
    dot_general x13 -> x0, matrix products: 31.6 us -> none  [the longest x1 8.98 us: local(): lifted = jnp.dot(normed, whole_up, preferred_element_type=jnp.float32)]
    all_gather x1 -> x0, blocking collectives: 12.8 us -> none  [collected_together(): both, at, found = (lax.all_gather(jnp.concatenate(lines), axis), 0, {})]
    slice x10 -> x4, local copies, waits for them, and re-layouts: 5.02 us -> 0.06 us  [local(): gate_up = jnp.concatenate([gate, up[:, 640:], up[:, :640]], axis=1)]
    reduce_max x4 -> x0, other arithmetic: 4.36 us -> none  [the longest x2 3.86 us: advance(): new_top = jnp.maximum(last_cum + top_log, jnp.max(log_end, axis=-1))]
  transfers between devices with their start and end apart: 3 -> 0, of which waited for: 3 -> 0; matrix products, arithmetic and copies ran while one was open for 2% -> 0% of each run, Pallas kernels for 0% -> 0%
where the time goes in v1:
time: 121 us
  Pallas kernels  114 us (94%)
  local copies, waits for them, and re-layouts  6.87 us (6%)
    pallas_call x1, Pallas kernels, local(): pl.pallas_call(cell_kernel, out_shape=jax.ShapeDtypeStruct(residual.shape...  114 us
    unnamed x7, local copies, waits for them, and re-layouts  3.54 us

profile of v1, /device:TPU:1, one launch (start us, length us, event | category | flops | bytes accessed | tf_op | source)
XLA Modules:
  0.0 120.7 jit_solution(12109450977299530518)
XLA Ops:
  0.0 0.0 copy-start.2
  0.0 0.7 copy-done.2
  0.7 0.6 reshape.6.hg_ref
  1.2 1.3 %reshape.7.ng_ref = bf16[1,2048]{1,0:T(2,128)(2,1)} reshape(bf16[2048]{0:T(1024)(128)(2,1)} %param.24) | data formatting | bytes 8192 | tf_op jit(solution)/shard_map/reshape | solution.py:578
  2.5 0.0 copy-start.1
  2.5 0.0 slice-start
  2.5 0.0 slice-start.1
  2.5 0.9 copy-done.1
  3.4 0.0 slice-done
  3.4 0.1 slice-done.1
  3.5 0.0 copy-start
  3.5 0.8 concatenate.3.gu_in
  4.2 0.1 copy-done
  4.4 0.6 pad.4.dn_in
  5.0 113.8 %shard_map.136 = bf16[1024,256]{1,0:T(8,128)(2,1)} custom-call(bf16[1024,128]{1,0:T(8,128)(2,1)} %q_ref.1, bf16[1024,128]{1,0:T(8,128)(2,1)} %k_ref.1, bf16[1024,256]{1,0:T(8,128)(2,1)} %v_ref.1, bf16[1024,256]{1,0:T(8,128)(2,1)} %og_ref.1, bf16[1,1024]{1,0:T(2,128)(2,1)} %ig_ref.1, bf16[1,1024]{1,0:T(2,128)(2,1)} %fg_ref.1, f32[1,1024]{1,0:T(1,128)} %ex_ref.1, ...), custom_call_target="tpu_custom_call" | custom-call | tf_op jit(solution)/shard_map/pallas_call | solution.py:558
  118.8 1.9 %copy.16 = bf16[1024,256]{1,0:T(8,128)(2,1)} copy(bf16[1024,256]{1,0:T(8,128)(2,1)} %shard_map.136) | data formatting | bytes 1048576
Async XLA Ops:
  0.0 0.7 copy-start.2
  2.5 0.9 copy-start.1
  2.5 0.9 slice-start
  2.5 0.9 slice-start.1
  3.5 0.9 copy-start

commit v2 on v1

v2 whole, which is shorter than its diff:
```python
import jax
import jax.numpy as jnp
from jax import lax
from jax.experimental import pallas as pl
from jax.experimental.pallas import tpu as pltpu
from jax.sharding import Mesh
from jax.sharding import PartitionSpec as P

MESH = pl.DeviceIdType.MESH
F32 = jnp.float32
BF16 = jnp.bfloat16
LOWEST_LOG = -1e30
EPSILON = 1e-06
NZ, NY, NX = 8, 4, 4
CHUNKS = 8
BLOCKS = 4
PER_BLOCK = CHUNKS // BLOCKS
BLOCK = 256


class Slots:
    def __init__(self):
        self.used = 0

    def take(self, count=1):
        first = self.used
        self.used += count
        return first


def running_rows(row, combine, identity):
    length = row.shape[1]
    lane = lax.broadcasted_iota(jnp.int32, row.shape, 1)
    step = 1
    while step < length:
        moved = jnp.where(lane >= step, pltpu.roll(row, step, 1), identity)
        row = combine(row, moved)
        step *= 2
    return row


def as_columns(row):
    return jnp.broadcast_to(row, (128, row.shape[1])).T


def wide(tile, copies):
    return jnp.concatenate([tile] * copies, axis=1)


def join(early, late):
    state_early, top_early, total_early = early
    state_late, top_late, total_late = late
    moved = top_early + total_late
    top = jnp.maximum(moved, top_late)
    left = wide(jnp.exp(moved - top), 2)
    right = wide(jnp.exp(top_late - top), 2)
    return (left * state_early + right * state_late, top, total_early + total_late)


def in_three(value):
    high = value.astype(BF16).astype(F32)
    middle = (value - high).astype(BF16).astype(F32)
    low = value - high - middle
    at = lax.broadcasted_iota(jnp.int32, (16, 128), 0)
    tile = jnp.where(at == 0, high, jnp.where(at == 1, middle, jnp.where(at == 2, low, 0.0)))
    return tile.astype(BF16)


def load_triple(ref, index):
    part = ref[index].astype(F32)
    scalars = part[32:33] + part[33:34] + part[34:35]
    return (part[0:32], scalars[:, 0:128], scalars[:, 128:256])


def store_triple(ref, index, triple):
    state, top, total = triple
    ref[index, 0:32, :] = state.astype(BF16)
    ref[index, 32:48, 0:128] = in_three(top)
    ref[index, 32:48, 128:256] = in_three(total)


def cell_kernel(
    q_in, k_in, v_in, og_in, ig_in, fg_in, ex_in, res_in, hg_in, wo_in, ng_in,
    gate_in, up_in, down_in,
    out_hbm,
    q_ref, k_ref, v_ref, og_ref, ig_ref, fg_ref, ex_ref, res_ref, hg_ref, wo_ref, ng_ref,
    gate_ref, up_ref, down_ref, out_ref,
    gu_all, dn_all, s1_src, s1_buf, s2_src, s2_buf, s3_src, s3_buf, state_ref,
    num_ref, pbuf, prcv, qbuf, rly, rsum, fin, sbuf, nbuf, hbuf,
    ssem, rsem, isem, osem,
):
    z, y, x, c = (lax.axis_index(a) for a in ("z", "y", "x", "c"))
    rows = q_ref.shape[0]
    chunk = rows // CHUNKS
    half = chunk // 2
    other = 1 - c
    x_at = [lax.rem(x + d, NX) for d in range(NX)]
    y_at = [lax.rem(y + d, NY) for d in range(NY)]
    z_at = [lax.rem(z + d, NZ) for d in range(NZ)]
    to_right, to_left, to_mate = {"x": x_at[1]}, {"x": x_at[3]}, {"c": other}
    y_right, y_left = {"y": y_at[1]}, {"y": y_at[3]}
    z_right, z_left = {"z": z_at[1]}, {"z": z_at[7]}
    stores, slots = [], Slots()

    def remote(src, dst, group, number, device):
        return pltpu.make_async_remote_copy(
            src_ref=src, dst_ref=dst, send_sem=ssem.at[group], recv_sem=rsem.at[number],
            device_id=device, device_id_type=MESH,
        )

    def send(src, dst, number, device, group):
        remote(src, dst, group, number, device).start()

    def arrived(dst, number):
        remote(dst, dst, 0, number, to_mate).wait_recv()

    def left(src, group):
        remote(src, src, group, 0, to_mate).wait_send()

    sums_out, gather_out, gu_out, dn_out, s1_out, s3_out, s2_out = (0, 1), 2, 3, 4, 5, 6, 7

    own = z * NY + y

    loads = {}
    for number, (name, src, dst) in enumerate((
        ("gate", gate_in, gate_ref), ("up", up_in, up_ref), ("down", down_in, down_ref),
        ("ig", ig_in, ig_ref), ("fg", fg_in, fg_ref), ("ex", ex_in, ex_ref),
        ("k", k_in, k_ref), ("v", v_in, v_ref), ("q", q_in, q_ref),
        ("hg", hg_in, hg_ref), ("ng", ng_in, ng_ref), ("og", og_in, og_ref),
        ("wo", wo_in, wo_ref), ("res", res_in, res_ref),
    )):
        loads[name] = pltpu.make_async_copy(src, dst, isem.at[number])

    def loaded(*names):
        for name in names:
            loads[name].wait()

    def enter():
        low = jnp.full((1, 128), LOWEST_LOG, F32)
        for j in range(NZ):
            store_triple(s2_buf, j, (jnp.zeros((32, 256), F32), low, jnp.zeros((1, 128), F32)))
        for copy in loads.values():
            copy.start()
        for device in partners:
            pl.semaphore_signal(barrier, inc=1, device_id=device, device_id_type=MESH)

    def lay_weights():
        loaded("gate", "up", "down")
        gate, up, down = gate_ref[...], up_ref[...], down_ref[...]
        gu_all[own, :, 0:640] = gate[:, 0:640]
        gu_all[own, :, 640:768] = jnp.concatenate([gate[:, 640:704], up[:, 640:704]], axis=1)
        gu_all[own, :, 768:1408] = up[:, 0:640]
        dn_all[own, :, 0:640] = down[:, 0:640]
        dn_all[own, :, 640:768] = jnp.concatenate(
            [down[:, 640:704], jnp.zeros((64, 64), BF16)], axis=1
        )

    barrier = pltpu.get_barrier_semaphore()
    partners = [to_right, to_left, to_mate]
    partners += [{"y": y_at[d]} for d in range(1, NY)] + [{"z": z_at[d]} for d in range(1, NZ)]

    def meet():
        pl.semaphore_wait(barrier, len(partners))

    gz_r, gz_l = slots.take(4), slots.take(4)
    gy_r, gy_l, gy_far = slots.take(8), slots.take(8), slots.take(1)
    dy = slots.take(3)
    dz_r, dz_l = slots.take(4), slots.take(3)
    z_order = [0, 7, 1, 6, 2, 5, 3, 4]
    piece = gu_all.shape[1] // 2

    def gu_z_send(step):
        if step == 0:
            at = gu_all.at[own]
            send(at, at, gz_r, z_right, gu_out)
            send(at, at, gz_l, z_left, gu_out)
        elif step < 3:
            for number, d, device in ((gz_r, NZ - step, z_right), (gz_l, step, z_left)):
                at = gu_all.at[z_at[d] * NY + y]
                send(at, at, number + step, device, gu_out)
        else:
            at = gu_all.at[z_at[5] * NY + y, pl.ds(0, piece)]
            send(at, at, gz_r + 3, z_right, gu_out)
            at = gu_all.at[z_at[3] * NY + y, pl.ds(piece, piece)]
            send(at, at, gz_l + 3, z_left, gu_out)

    def gu_z_wait(step):
        if step < 3:
            arrived(gu_all.at[z_at[7 - step] * NY + y], gz_r + step)
            arrived(gu_all.at[z_at[1 + step] * NY + y], gz_l + step)
        else:
            arrived(gu_all.at[z_at[4] * NY + y, pl.ds(0, piece)], gz_r + 3)
            arrived(gu_all.at[z_at[4] * NY + y, pl.ds(piece, piece)], gz_l + 3)

    def gu_y_send(k):
        at = gu_all.at[z_at[z_order[k]] * NY + y]
        send(at, at, gy_r + k, y_right, gu_out)
        send(at, at, gy_l + k, y_left, gu_out)

    def gu_y_forward(k):
        block = z_at[z_order[k]] * NY
        arrived(gu_all.at[block + y_at[3]], gy_r + k)
        at = gu_all.at[block + y_at[3], pl.ds(0, piece)]
        send(at, at, gy_far, y_right, gu_out)
        arrived(gu_all.at[block + y_at[1]], gy_l + k)
        at = gu_all.at[block + y_at[1], pl.ds(piece, piece)]
        send(at, at, gy_far, y_left, gu_out)

    def gu_y_wait():
        arrived(gu_all.at[pl.ds(0, NZ)], gy_far)

    def dn_y_send():
        at = dn_all.at[own]
        send(at, at, dy, y_right, dn_out)
        send(at, at, dy + 1, y_left, dn_out)

    def dn_y_forward():
        arrived(dn_all.at[z * NY + y_at[3]], dy)
        at = dn_all.at[z * NY + y_at[3], pl.ds(0, piece)]
        send(at, at, dy + 2, y_right, dn_out)
        arrived(dn_all.at[z * NY + y_at[1]], dy + 1)
        at = dn_all.at[z * NY + y_at[1], pl.ds(piece, piece)]
        send(at, at, dy + 2, y_left, dn_out)

    def dn_y_wait():
        arrived(dn_all.at[z * NY + y_at[2]], dy + 2)

    def dn_z_send(step):
        if step < 3:
            for number, d, device in ((dz_r, (NZ - step) % NZ, z_right), (dz_l, step, z_left)):
                at = dn_all.at[pl.ds(z_at[d] * NY, NY)]
                send(at, at, number + step, device, dn_out)
        else:
            at = dn_all.at[pl.ds(z_at[5] * NY, 2)]
            send(at, at, dz_r + 3, z_right, dn_out)
            at = dn_all.at[pl.ds(z_at[3] * NY + 2, 2)]
            send(at, at, dz_r + 3, z_left, dn_out)

    def dn_z_wait(step):
        if step < 3:
            arrived(dn_all.at[pl.ds(z_at[7 - step] * NY, NY)], dz_r + step)
            arrived(dn_all.at[pl.ds(z_at[1 + step] * NY, NY)], dz_l + step)
        else:
            arrived(dn_all.at[pl.ds(z_at[4] * NY, NY)], dz_r + 3)

    def gates():
        loaded("ig", "fg", "ex")
        logits = fg_ref[...].astype(F32)
        log_forget = jnp.minimum(logits, 0.0) - jnp.log1p(jnp.exp(-jnp.abs(logits))) + ex_ref[...]
        cum = running_rows(log_forget, jnp.add, 0.0)
        lead = ig_ref[...].astype(F32) - cum
        return cum, lead, running_rows(lead, jnp.maximum, -jnp.inf)

    s1, s2, s3 = slots.take(), slots.take(NZ - 1) - 1, slots.take()

    def end_parts():
        loaded("k", "v")
        last_cum, last_lead = cum[:, rows - 1 :], top_run[:, rows - 1 :]
        weight = as_columns(jnp.exp(lead - last_lead))
        scaled = (k_ref[...].astype(F32) * weight).astype(BF16)
        end_state = lax.dot_general(
            scaled, v_ref[...], (((0,), (0,)), ((), ())), preferred_element_type=F32
        )
        end_top = jnp.broadcast_to(last_cum + last_lead, (1, 128))
        end_total = jnp.broadcast_to(last_cum, (1, 128))
        for p in range(NY):
            store_triple(s1_src, p, (end_state[p * 32 : p * 32 + 32], end_top, end_total))
        s1_buf[y] = s1_src[y]

    def send_parts():
        for d in range(1, NY):
            send(s1_src.at[y_at[d]], s1_buf.at[y], s1, {"y": y_at[d]}, s1_out)

    step_rows = 256

    def local_rows(i):
        r0 = i * step_rows
        top_tile = top_cols[r0 : r0 + step_rows]
        parts = None
        for j in range(i + 1):
            s0 = j * step_rows
            scores = lax.dot_general(
                q_ref[r0 : r0 + step_rows], k_ref[s0 : s0 + step_rows],
                (((1,), (1,)), ((), ())), preferred_element_type=F32,
            )
            log_weight = lead[:, s0 : s0 + step_rows] - wide(top_tile, step_rows // 128)
            if i == j:
                at_row = lax.broadcasted_iota(jnp.int32, (step_rows, step_rows), 0)
                at_col = lax.broadcasted_iota(jnp.int32, (step_rows, step_rows), 1)
                log_weight = jnp.where(at_col <= at_row, log_weight, -jnp.inf)
            scores = (scores * (128.0**-0.5) * jnp.exp(log_weight)).astype(BF16)
            term = jnp.dot(scores, v_ref[s0 : s0 + step_rows], preferred_element_type=F32)
            parts = term if parts is None else parts + term
        num_ref[r0 : r0 + step_rows, :] = parts

    def state_copy(d):
        return remote(s2_src.at[0], s2_buf.at[z], s2_out + d - 1, s2 + d, {"z": z_at[d]})

    def y_states():
        arrived(s1_buf.at[pl.ds(0, NY - 1)], s1)
        inside = [load_triple(s1_buf, 0)]
        for j in range(1, NY):
            inside.append(join(inside[-1], load_triple(s1_buf, j)))
        store_triple(s2_src, 0, inside[-1])
        for d in range(1, NZ):

            @pl.when(z + d < NZ)
            def _(d=d):
                state_copy(d).start()

        return inside

    def z_states():
        for d in range(1, NZ):

            @pl.when(z - d >= 0)
            def _(d=d):
                arrived(s2_buf.at[z_at[NZ - d]], s2 + d)

        before = load_triple(s2_buf, 0)
        for j in range(1, NZ):
            before = join(before, load_triple(s2_buf, j))
        store_triple(s3_src, 0, before)
        for j in range(1, NY):
            store_triple(s3_src, j, join(before, inside[j - 1]))
        for d in range(1, NY):
            send(s3_src.at[y_at[d]], s3_buf.at[y], s3, {"y": y_at[d]}, s3_out)
        s3_buf[y] = s3_src[y]

    def carried():
        arrived(s3_buf.at[pl.ds(0, NY - 1)], s3)
        for p in range(NY):
            state_ref[p * 32 : p * 32 + 32, :] = s3_buf[p, 0:32, :]
        return load_triple(s3_buf, 0)[1]

    enter()
    lay_weights()
    cum, lead, top_run = gates()
    end_parts()
    meet()
    send_parts()
    gu_z_send(0)
    top_cols = as_columns(top_run)
    loaded("q", "hg", "ng", "og", "wo", "res")
    head_gain = hg_ref[...].astype(F32).reshape(1, 256)
    feed_gain = ng_ref[...].astype(F32).reshape(1, 2048)
    for i in range(4):
        local_rows(i)
    inside = y_states()
    dn_y_send()
    gu_y_send(0)
    gu_z_wait(0)
    gu_z_send(1)
    z_states()
    gu_y_send(1)
    gu_y_send(2)
    dn_y_forward()
    carried_top = carried()

    def reduce_slots():
        return [slots.take(4) for _ in range(CHUNKS)]

    sums = (reduce_slots(), reduce_slots())
    gathers = [slots.take(4) for _ in range(CHUNKS)]

    def swap_send(a, i):
        send(pbuf.at[a, i, other], prcv.at[a, i], sums[a][i], to_mate, sums_out[a])

    def swap_join(a, i):
        n = sums[a][i]
        arrived(prcv.at[a, i], n)
        for j in range(NX):
            both = pbuf[a, i, c, j].astype(F32) + prcv[a, i, j].astype(F32)
            qbuf[a, i, j] = both.astype(BF16)
        top, low = pl.ds(0, half), pl.ds(half, half)
        send(qbuf.at[a, i, x_at[2], top], rly.at[a, i, 0], n + 1, to_right, sums_out[a])
        send(qbuf.at[a, i, x_at[2], low], rly.at[a, i, 1], n + 2, to_left, sums_out[a])
        send(qbuf.at[a, i, x_at[1], low], fin.at[a, i, 0, 1], n + 3, to_right, sums_out[a])
        send(qbuf.at[a, i, x_at[3], top], fin.at[a, i, 1, 0], n + 3, to_left, sums_out[a])

    def relay(a, i):
        n = sums[a][i]
        arrived(rly.at[a, i, 0], n + 1)
        added = rly[a, i, 0].astype(F32) + qbuf[a, i, x_at[1], 0:half].astype(F32)
        rsum[a, i, 0] = added.astype(BF16)
        send(rsum.at[a, i, 0], fin.at[a, i, 0, 0], n + 3, to_right, sums_out[a])
        arrived(rly.at[a, i, 1], n + 2)
        added = rly[a, i, 1].astype(F32) + qbuf[a, i, x_at[3], half:].astype(F32)
        rsum[a, i, 1] = added.astype(BF16)
        send(rsum.at[a, i, 1], fin.at[a, i, 1, 1], n + 3, to_left, sums_out[a])

    def total(a, i):
        n = sums[a][i]
        arrived(fin.at[a, i], n + 3)
        found = []
        for h in range(2):
            own = qbuf[a, i, x, h * half : h * half + half].astype(F32)
            found.append(own + fin[a, i, 0, h].astype(F32) + fin[a, i, 1, h].astype(F32))
        return jnp.concatenate(found, axis=0)

    def gated_block(g):
        part = pl.ds(g * BLOCK, BLOCK)
        run = top_cols[g * BLOCK : g * BLOCK + BLOCK]
        top = jnp.maximum(run, carried_top)
        keep = wide(jnp.exp(run - top), 2)
        enter = wide(jnp.exp(carried_top - top) * (128.0**-0.5), 2)
        earlier = jnp.dot(q_ref[part], state_ref[...], preferred_element_type=F32)
        memory = keep * num_ref[part] + enter * earlier
        mean = jnp.mean(memory * memory, axis=1, keepdims=True)
        opened = jax.nn.sigmoid(og_ref[part].astype(F32))
        gated = memory * lax.rsqrt(mean + EPSILON) * head_gain * opened
        gated = gated.astype(BF16)
        place(0, g, lambda b: jnp.dot(
            gated, wo_ref[:, b * 256 : b * 256 + 256], preferred_element_type=F32
        ))

    def place(a, g, term):
        for b in range(2 * NX):
            found = term(b).astype(BF16)
            for i in range(PER_BLOCK):
                pbuf[a, g * PER_BLOCK + i, b % 2, b // 2] = found[i * chunk : i * chunk + chunk]
        for i in range(PER_BLOCK):
            swap_send(a, g * PER_BLOCK + i)

    def stream_chunk(i):
        n = gathers[i]
        summed = total(0, i) + res_ref[pl.ds(i * chunk, chunk)].astype(F32)
        sbuf[i, c, x] = summed.astype(BF16)
        at = sbuf.at[i, c, x]
        send(at, at, n, to_right, gather_out)
        send(at, at, n + 1, to_left, gather_out)
        send(at, at, n + 3, to_mate, gather_out)

    def spread_chunk(i):
        n = gathers[i]
        for number, d, first, device in ((n, 3, 0, to_right), (n + 1, 1, half, to_left)):
            at = sbuf.at[i, c, x_at[d]]
            arrived(at, number)
            part = sbuf.at[i, c, x_at[d], pl.ds(first, half)]
            send(part, part, n + 2, device, gather_out)
            send(at, at, n + 3, to_mate, gather_out)

    def far_chunk(i):
        n = gathers[i]
        at = sbuf.at[i, c, x_at[2]]
        arrived(at, n + 2)
        send(at, at, n + 3, to_mate, gather_out)

    def normed_chunk(i):
        arrived(sbuf.at[i, other], gathers[i] + 3)
        square = jnp.zeros((chunk, 256), F32)
        for b in range(2 * NX):
            part = sbuf[i, b % 2, b // 2].astype(F32)
            square = square + part * part
        mean = jnp.sum(square, axis=1, keepdims=True) * (1.0 / (2 * NX * 256))
        scale = lax.rsqrt(mean + EPSILON)
        for b in range(2 * NX):
            cols = slice(b * 256, b * 256 + 256)
            part = sbuf[i, b % 2, b // 2].astype(F32)
            nbuf[pl.ds(i * chunk, chunk), cols] = (part * scale * feed_gain[:, cols]).astype(BF16)

    def pump(tick):
        if tick == 0:
            gu_z_wait(1)
            gu_z_send(2)
            gu_y_send(3)
        elif tick == 1:
            dn_y_wait()
            dn_z_send(0)
            gu_y_send(4)
        elif tick == 2:
            gu_z_wait(2)
            gu_z_send(3)
            gu_y_send(5)
            gu_y_send(6)
        elif tick == 3:
            gu_y_forward(0)
            gu_y_forward(1)
        elif tick == 4:
            dn_z_wait(0)
            dn_z_send(1)
            gu_z_wait(3)
            gu_y_send(7)
        elif tick == 5:
            gu_y_forward(2)
            gu_y_forward(3)
        elif tick == 6:
            dn_z_wait(1)
            dn_z_send(2)
            gu_y_forward(4)
        elif tick == 7:
            gu_y_forward(5)
        elif tick == 8:
            gu_y_forward(6)
        elif tick == 9:
            dn_z_wait(2)
            dn_z_send(3)
            gu_y_forward(7)

    def run(stages, pump=None):
        for tick in range(CHUNKS + max(lag for lag, _ in stages)):
            for lag, stage in stages:
                if 0 <= tick - lag < CHUNKS:
                    stage(tick - lag)
            if pump is not None:
                pump(tick)

    def first_of_block(stage):
        def begin(i):
            if i % PER_BLOCK == 0:
                stage(i // PER_BLOCK)

        return begin

    def join_first(i):
        swap_join(0, i)

    def relay_first(i):
        relay(0, i)

    run(
        (
            (0, first_of_block(gated_block)), (1, join_first), (2, relay_first),
            (3, stream_chunk), (4, spread_chunk), (5, far_chunk), (6, normed_chunk),
        ),
        pump,
    )

    def silu(v):
        return v / (1.0 + jnp.exp(-v))

    def up_block(g):
        lines = nbuf[pl.ds(g * BLOCK, BLOCK)]
        part = pl.ds(g * BLOCK, BLOCK)

        def up_cols(col, width):
            weights = gu_all[:, :, col : col + width].reshape(NZ * NY * 64, width)
            return jnp.dot(lines, weights, preferred_element_type=F32)

        for col in (0, 256):
            hidden = silu(up_cols(col, 256)) * up_cols(768 + col, 256)
            hbuf[part, col : col + 256] = hidden.astype(BF16)
        tail = up_cols(512, 256)
        hidden = silu(tail[:, :128]) * up_cols(1280, 128)
        hbuf[part, 512:640] = hidden.astype(BF16)
        mixed_tile = tail[:, 128:]
        hidden = silu(mixed_tile) * pltpu.roll(mixed_tile, 64, 1)
        lane = lax.broadcasted_iota(jnp.int32, hidden.shape, 1)
        hbuf[part, 640:768] = jnp.where(lane < 64, hidden, 0.0).astype(BF16)

    def down_block(g):
        def term(b):
            weights = dn_all[b * 4 : b * 4 + 4].reshape(256, dn_all.shape[2])
            return lax.dot_general(
                hbuf[pl.ds(g * BLOCK, BLOCK)], weights, (((1,), (1,)), ((), ())),
                preferred_element_type=F32,
            )

        place(1, g, term)

    def mixed_chunk(i):
        summed = sbuf[i, c, x].astype(F32) + 0.5 * total(1, i)
        part = pl.ds(i * chunk, chunk)
        out_ref[part] = summed.astype(BF16)
        stores.append(pltpu.make_async_copy(out_ref.at[part], out_hbm.at[part], osem.at[i]))
        stores[-1].start()

    def feed_block(g):
        if g == 0:
            gu_y_wait()
        up_block(g)
        if g == 0:
            dn_z_wait(3)
        down_block(g)

    def join_last(i):
        swap_join(1, i)

    def relay_last(i):
        relay(1, i)

    run(((0, first_of_block(feed_block)), (1, join_last), (3, relay_last), (5, mixed_chunk)))

    def drain():
        for copy in stores:
            copy.wait()
        for group in (*sums_out, gather_out):
            left(sbuf.at[pl.ds(0, 7)], group)
        left(gu_all.at[pl.ds(0, 31)], gu_out)
        left(dn_all.at[pl.ds(0, 31)], dn_out)
        left(s1_buf.at[pl.ds(0, NY - 1)], s1_out)
        left(s3_buf.at[pl.ds(0, NY - 1)], s3_out)
        for d in range(1, NZ):

            @pl.when(z + d < NZ)
            def _(d=d):
                state_copy(d).wait_send()

    drain()
    assert slots.used <= RECEIVES


RECEIVES, SENDS = 144, 14


def local(
    queries,
    cell_key_rows,
    cell_value_rows,
    output_gate_logits,
    input_gate_logits,
    forget_gate_logits,
    forget_extra_term,
    residual,
    head_norm_gain,
    cell_output_weight,
    feedforward_norm_gain,
    gate_projection_weight,
    up_projection_weight,
    down_projection_weight,
):
    rows = queries.shape[0]
    chunk = rows // CHUNKS
    half = chunk // 2
    vmem = pltpu.VMEM
    arguments = (
        queries,
        cell_key_rows,
        cell_value_rows,
        output_gate_logits,
        input_gate_logits,
        forget_gate_logits,
        forget_extra_term,
        residual,
        head_norm_gain,
        cell_output_weight,
        feedforward_norm_gain,
        gate_projection_weight,
        up_projection_weight,
        down_projection_weight.T,
    )
    scratch = [vmem(a.shape, a.dtype) for a in arguments] + [
        vmem(residual.shape, BF16),
        vmem((NZ * NY, 64, 1408), BF16),
        vmem((NZ * NY, 64, 768), BF16),
        vmem((NY, 48, 256), BF16),
        vmem((NY, 48, 256), BF16),
        vmem((1, 48, 256), BF16),
        vmem((NZ, 48, 256), BF16),
        vmem((NY, 48, 256), BF16),
        vmem((NY, 48, 256), BF16),
        vmem((128, 256), BF16),
        vmem((rows, 256), F32),
        vmem((2, CHUNKS, 2, NX, chunk, 256), BF16),
        vmem((2, CHUNKS, NX, chunk, 256), BF16),
        vmem((2, CHUNKS, NX, chunk, 256), BF16),
        vmem((2, CHUNKS, 2, half, 256), BF16),
        vmem((2, CHUNKS, 2, half, 256), BF16),
        vmem((2, CHUNKS, 2, 2, half, 256), BF16),
        vmem((CHUNKS, 2, NX, chunk, 256), BF16),
        vmem((rows, 2048), BF16),
        vmem((rows, 768), BF16),
        pltpu.SemaphoreType.DMA((SENDS,)),
        pltpu.SemaphoreType.DMA((RECEIVES,)),
        pltpu.SemaphoreType.DMA((len(arguments),)),
        pltpu.SemaphoreType.DMA((CHUNKS,)),
    ]
    return pl.pallas_call(
        cell_kernel,
        out_shape=jax.ShapeDtypeStruct(residual.shape, BF16),
        in_specs=[pl.BlockSpec(memory_space=pl.ANY)] * 14,
        out_specs=pl.BlockSpec(memory_space=pl.ANY),
        scratch_shapes=scratch,
        compiler_params=pltpu.CompilerParams(
            collective_id=0, has_side_effects=True, vmem_limit_bytes=62 * 1024 * 1024
        ),
    )(*arguments)


def solution(mesh):
    torus = Mesh(mesh.devices.reshape(NZ, NY, NX, 2), ("z", "y", "x", "c"))
    seq, head = ("z", "y"), ("x", "c")
    in_specs = (
        P(seq, head),
        P(seq, head),
        P(seq, head),
        P(seq, head),
        P(head, seq),
        P(head, seq),
        P(head, seq),
        P(seq, head),
        P(head),
        P(head, None),
        P(),
        P(seq, head),
        P(seq, head),
        P(head, seq),
    )
    return jax.shard_map(
        local, mesh=torus, in_specs=in_specs, out_specs=P(seq, head), check_vma=False
    )
```

time: 121 us -> 104 us (0.86)
  Pallas kernels: 114 us -> 102 us
  local copies, waits for them, and re-layouts: 6.87 us -> 1.87 us
    pallas_call x1, Pallas kernels: 114 us -> 102 us  [local(): pl.pallas_call(cell_kernel, out_shape=jax.ShapeDtypeStruct(residual.shape...]
    reshape x2 -> x0, local copies, waits for them, and re-layouts: 1.86 us -> none  [the longest x1 1.29 us: local(): feedforward_norm_gain.reshape(1, -1)]
    unnamed x7 -> x1, local copies, waits for them, and re-layouts: 3.54 us -> 1.87 us
where the time goes in v2:
time: 104 us; the launch traced here: 103 us
  Pallas kernels  102 us (98%)
  local copies, waits for them, and re-layouts  1.87 us (2%)
    pallas_call x1, Pallas kernels, local(): pl.pallas_call(cell_kernel, out_shape=jax.ShapeDtypeStruct(residual.shape...  102 us

profile of v2, /device:TPU:1, one launch (start us, length us, event | category | flops | bytes accessed | tf_op | source)
XLA Modules:
  0.0 103.4 jit_solution(4106548579289496465)
XLA Ops:
  0.0 101.5 %shard_map.136 = bf16[1024,256]{1,0:T(8,128)(2,1)} custom-call(bf16[1024,128]{1,0:T(8,128)(2,1)} %q_in.1, bf16[1024,128]{1,0:T(8,128)(2,1)} %k_in.1, bf16[1024,256]{1,0:T(8,128)(2,1)} %v_in.1, bf16[1024,256]{1,0:T(8,128)(2,1)} %og_in.1, bf16[1,1024]{1,0:T(2,128)(2,1)} %ig_in.1, bf16[1,1024]{1,0:T(2,128)(2,1)} %fg_in.1, f32[1,1024]{1,0:T(1,128)} %ex_in.1, ...), custom_call_target="tpu_custom_call" | custom-call | tf_op jit(solution)/shard_map/pallas_call | solution.py:668
  101.5 1.9 %copy.16 = bf16[1024,256]{1,0:T(8,128)(2,1)} copy(bf16[1024,256]{1,0:T(8,128)(2,1)} %shard_map.136) | data formatting | bytes 1048576

commit v3 on v2

--- a/solution.py
+++ b/solution.py
@@ -16,6 +16,7 @@
 BLOCKS = 4
 PER_BLOCK = CHUNKS // BLOCKS
 BLOCK = 256
+EARLY = 2
 
 
 class Slots:
@@ -117,7 +118,7 @@
     def left(src, group):
         remote(src, src, group, 0, to_mate).wait_send()
 
-    sums_out, gather_out, gu_out, dn_out, s1_out, s3_out, s2_out = (0, 1), 2, 3, 4, 5, 6, 7
+    sums_out, gather_out, gu_out, dn_out, s1_out, s3_out, low_out, s2_out = (0, 1), 2, 3, 4, 5, 6, 7, 8
 
     own = z * NY + y
 
@@ -162,86 +163,93 @@
     def meet():
         pl.semaphore_wait(barrier, len(partners))
 
-    gz_r, gz_l = slots.take(4), slots.take(4)
-    gy_r, gy_l, gy_far = slots.take(8), slots.take(8), slots.take(1)
-    dy = slots.take(3)
-    dz_r, dz_l = slots.take(4), slots.take(3)
     z_order = [0, 7, 1, 6, 2, 5, 3, 4]
-    piece = gu_all.shape[1] // 2
-
-    def gu_z_send(step):
-        if step == 0:
-            at = gu_all.at[own]
-            send(at, at, gz_r, z_right, gu_out)
-            send(at, at, gz_l, z_left, gu_out)
-        elif step < 3:
-            for number, d, device in ((gz_r, NZ - step, z_right), (gz_l, step, z_left)):
-                at = gu_all.at[z_at[d] * NY + y]
-                send(at, at, number + step, device, gu_out)
-        else:
-            at = gu_all.at[z_at[5] * NY + y, pl.ds(0, piece)]
-            send(at, at, gz_r + 3, z_right, gu_out)
-            at = gu_all.at[z_at[3] * NY + y, pl.ds(piece, piece)]
-            send(at, at, gz_l + 3, z_left, gu_out)
-
-    def gu_z_wait(step):
-        if step < 3:
-            arrived(gu_all.at[z_at[7 - step] * NY + y], gz_r + step)
-            arrived(gu_all.at[z_at[1 + step] * NY + y], gz_l + step)
-        else:
-            arrived(gu_all.at[z_at[4] * NY + y, pl.ds(0, piece)], gz_r + 3)
-            arrived(gu_all.at[z_at[4] * NY + y, pl.ds(piece, piece)], gz_l + 3)
-
-    def gu_y_send(k):
-        at = gu_all.at[z_at[z_order[k]] * NY + y]
-        send(at, at, gy_r + k, y_right, gu_out)
-        send(at, at, gy_l + k, y_left, gu_out)
-
-    def gu_y_forward(k):
-        block = z_at[z_order[k]] * NY
-        arrived(gu_all.at[block + y_at[3]], gy_r + k)
-        at = gu_all.at[block + y_at[3], pl.ds(0, piece)]
-        send(at, at, gy_far, y_right, gu_out)
-        arrived(gu_all.at[block + y_at[1]], gy_l + k)
-        at = gu_all.at[block + y_at[1], pl.ds(piece, piece)]
-        send(at, at, gy_far, y_left, gu_out)
-
-    def gu_y_wait():
-        arrived(gu_all.at[pl.ds(0, NZ)], gy_far)
-
-    def dn_y_send():
-        at = dn_all.at[own]
-        send(at, at, dy, y_right, dn_out)
-        send(at, at, dy + 1, y_left, dn_out)
-
-    def dn_y_forward():
-        arrived(dn_all.at[z * NY + y_at[3]], dy)
-        at = dn_all.at[z * NY + y_at[3], pl.ds(0, piece)]
-        send(at, at, dy + 2, y_right, dn_out)
-        arrived(dn_all.at[z * NY + y_at[1]], dy + 1)
-        at = dn_all.at[z * NY + y_at[1], pl.ds(piece, piece)]
-        send(at, at, dy + 2, y_left, dn_out)
-
-    def dn_y_wait():
-        arrived(dn_all.at[z * NY + y_at[2]], dy + 2)
-
-    def dn_z_send(step):
-        if step < 3:
-            for number, d, device in ((dz_r, (NZ - step) % NZ, z_right), (dz_l, step, z_left)):
-                at = dn_all.at[pl.ds(z_at[d] * NY, NY)]
-                send(at, at, number + step, device, dn_out)
-        else:
-            at = dn_all.at[pl.ds(z_at[5] * NY, 2)]
-            send(at, at, dz_r + 3, z_right, dn_out)
-            at = dn_all.at[pl.ds(z_at[3] * NY + 2, 2)]
-            send(at, at, dz_r + 3, z_left, dn_out)
-
-    def dn_z_wait(step):
-        if step < 3:
-            arrived(dn_all.at[pl.ds(z_at[7 - step] * NY, NY)], dz_r + step)
-            arrived(dn_all.at[pl.ds(z_at[1 + step] * NY, NY)], dz_l + step)
-        else:
-            arrived(dn_all.at[pl.ds(z_at[4] * NY, NY)], dz_r + 3)
+
+    class ZFirst:
+        def __init__(self, ref, count, group):
+            self.ref, self.count, self.group = ref, count, group
+            self.along_z, self.along_y, self.far = slots.take(4), slots.take(NZ), slots.take()
+
+        def part(self, block, first, count):
+            return self.ref.at[block, pl.ds(first, count)]
+
+        def pass_on(self, at, number, device):
+            send(at, at, number, device, self.group)
+
+        def taken(self, blocks, number):
+            arrived(self.ref.at[pl.ds(0, blocks), pl.ds(0, self.count)], number)
+
+        def z_send(self, step):
+            half_rows = self.count // 2
+            for d, first, device in (((NZ - step) % NZ, 0, z_right), (step, half_rows, z_left)):
+                block = z_at[d] * NY + y
+                whole = (0, self.count) if step < 3 else (first, half_rows)
+                self.pass_on(self.part(block, *whole), self.along_z + step, device)
+
+        def z_wait(self, step):
+            self.taken(2 if step < 3 else 1, self.along_z + step)
+
+        def y_send(self, k):
+            at = self.part(z_at[z_order[k]] * NY + y, 0, self.count)
+            self.pass_on(at, self.along_y + k, y_right)
+            self.pass_on(at, self.along_y + k, y_left)
+
+        def y_forward(self, k):
+            self.taken(2, self.along_y + k)
+            block, half_rows = z_at[z_order[k]] * NY, self.count // 2
+            self.pass_on(self.part(block + y_at[3], 0, half_rows), self.far, y_right)
+            self.pass_on(self.part(block + y_at[1], half_rows, half_rows), self.far, y_left)
+
+        def y_wait(self):
+            self.taken(NZ, self.far)
+
+    class YFirst:
+        def __init__(self, ref, first, count, group):
+            self.ref, self.first, self.count, self.group = ref, first, count, group
+            self.along_y, self.far, self.along_z = slots.take(), slots.take(), slots.take(7)
+
+        def pass_on(self, at, number, device):
+            send(at, at, number, device, self.group)
+
+        def taken(self, blocks, number):
+            arrived(self.ref.at[pl.ds(0, blocks), pl.ds(self.first, self.count)], number)
+
+        def y_send(self):
+            at = self.ref.at[own, pl.ds(self.first, self.count)]
+            self.pass_on(at, self.along_y, y_right)
+            self.pass_on(at, self.along_y, y_left)
+
+        def y_forward(self):
+            self.taken(2, self.along_y)
+            half_rows = self.count // 2
+            at = self.ref.at[z * NY + y_at[3], pl.ds(self.first, half_rows)]
+            self.pass_on(at, self.far, y_right)
+            at = self.ref.at[z * NY + y_at[1], pl.ds(self.first + half_rows, half_rows)]
+            self.pass_on(at, self.far, y_left)
+
+        def y_wait(self):
+            self.taken(1, self.far)
+
+        def pair(self, d, part):
+            return self.ref.at[pl.ds(z_at[d] * NY + 2 * part, 2), pl.ds(self.first, self.count)]
+
+        def z_send(self, step, part):
+            if step < 3:
+                number = self.along_z + 2 * step + part
+                self.pass_on(self.pair((NZ - step) % NZ, part), number, z_right)
+                self.pass_on(self.pair(step, part), number, z_left)
+            elif part == 0:
+                self.pass_on(self.pair(5, 0), self.along_z + 6, z_right)
+            else:
+                self.pass_on(self.pair(3, 1), self.along_z + 6, z_left)
+
+        def z_wait(self, step, part):
+            self.taken(4, self.along_z + 2 * step + part)
+
+    gu_rows = gu_all.shape[1] // 2
+    top_gu = ZFirst(gu_all, gu_rows, gu_out)
+    low_gu = YFirst(gu_all, gu_rows, gu_rows, low_out)
+    dn = ZFirst(dn_all, dn_all.shape[1], dn_out)
 
     def gates():
         loaded("ig", "fg", "ex")
@@ -339,7 +347,9 @@
     end_parts()
     meet()
     send_parts()
-    gu_z_send(0)
+    top_gu.z_send(0)
+    low_gu.y_send()
+    top_gu.y_send(0)
     top_cols = as_columns(top_run)
     loaded("q", "hg", "ng", "og", "wo", "res")
     head_gain = hg_ref[...].astype(F32).reshape(1, 256)
@@ -347,14 +357,14 @@
     for i in range(4):
         local_rows(i)
     inside = y_states()
-    dn_y_send()
-    gu_y_send(0)
-    gu_z_wait(0)
-    gu_z_send(1)
+    top_gu.z_wait(0)
+    top_gu.z_send(1)
+    dn.z_send(0)
+    top_gu.y_send(1)
     z_states()
-    gu_y_send(1)
-    gu_y_send(2)
-    dn_y_forward()
+    low_gu.y_forward()
+    top_gu.y_send(2)
+    dn.y_send(0)
     carried_top = carried()
 
     def reduce_slots():
@@ -375,6 +385,12 @@
         top, low = pl.ds(0, half), pl.ds(half, half)
         send(qbuf.at[a, i, x_at[2], top], rly.at[a, i, 0], n + 1, to_right, sums_out[a])
         send(qbuf.at[a, i, x_at[2], low], rly.at[a, i, 1], n + 2, to_left, sums_out[a])
+        if i < EARLY or (a == 1 and i == CHUNKS - 1):
+            direct(a, i)
+
+    def direct(a, i):
+        n = sums[a][i]
+        top, low = pl.ds(0, half), pl.ds(half, half)
         send(qbuf.at[a, i, x_at[1], low], fin.at[a, i, 0, 1], n + 3, to_right, sums_out[a])
         send(qbuf.at[a, i, x_at[3], top], fin.at[a, i, 1, 0], n + 3, to_left, sums_out[a])
 
@@ -388,6 +404,8 @@
         added = rly[a, i, 1].astype(F32) + qbuf[a, i, x_at[3], half:].astype(F32)
         rsum[a, i, 1] = added.astype(BF16)
         send(rsum.at[a, i, 1], fin.at[a, i, 1, 1], n + 3, to_left, sums_out[a])
+        if i >= EARLY and not (a == 1 and i == CHUNKS - 1):
+            direct(a, i)
 
     def total(a, i):
         n = sums[a][i]
@@ -410,17 +428,21 @@
         opened = jax.nn.sigmoid(og_ref[part].astype(F32))
         gated = memory * lax.rsqrt(mean + EPSILON) * head_gain * opened
         gated = gated.astype(BF16)
-        place(0, g, lambda b: jnp.dot(
-            gated, wo_ref[:, b * 256 : b * 256 + 256], preferred_element_type=F32
-        ))
+        def term(j, core):
+            columns = pl.ds(pl.multiple_of((2 * j + core) * 256, 256), 256)
+            return jnp.dot(gated, wo_ref[:, columns], preferred_element_type=F32)
+
+        place(0, g, term)
 
     def place(a, g, term):
-        for b in range(2 * NX):
-            found = term(b).astype(BF16)
-            for i in range(PER_BLOCK):
-                pbuf[a, g * PER_BLOCK + i, b % 2, b // 2] = found[i * chunk : i * chunk + chunk]
-        for i in range(PER_BLOCK):
-            swap_send(a, g * PER_BLOCK + i)
+        for core in (other, c):
+            for j in range(NX):
+                found = term(j, core).astype(BF16)
+                for i in range(PER_BLOCK):
+                    pbuf[a, g * PER_BLOCK + i, core, j] = found[i * chunk : i * chunk + chunk]
+            if core is other:
+                for i in range(PER_BLOCK):
+                    swap_send(a, g * PER_BLOCK + i)
 
     def stream_chunk(i):
         n = gathers[i]
@@ -461,41 +483,83 @@
 
     def pump(tick):
         if tick == 0:
-            gu_z_wait(1)
-            gu_z_send(2)
-            gu_y_send(3)
+            top_gu.z_wait(1)
+            top_gu.z_send(2)
+            low_gu.y_wait()
+            low_gu.z_send(0, 0)
+            top_gu.y_send(3)
+            top_gu.y_send(4)
+            dn.z_wait(0)
+            dn.z_send(1)
         elif tick == 1:
-            dn_y_wait()
-            dn_z_send(0)
-            gu_y_send(4)
+            low_gu.z_send(0, 1)
         elif tick == 2:
-            gu_z_wait(2)
-            gu_z_send(3)
-            gu_y_send(5)
-            gu_y_send(6)
+            top_gu.y_forward(0)
+            dn.y_send(1)
         elif tick == 3:
-            gu_y_forward(0)
-            gu_y_forward(1)
+            top_gu.z_wait(2)
+            top_gu.z_send(3)
+            top_gu.y_send(5)
+            top_gu.y_send(6)
+            top_gu.y_forward(1)
         elif tick == 4:
-            dn_z_wait(0)
-            dn_z_send(1)
-            gu_z_wait(3)
-            gu_y_send(7)
+            dn.z_wait(1)
+            dn.z_send(2)
+            dn.y_send(2)
+            top_gu.y_forward(2)
+            top_gu.y_forward(3)
+            low_gu.z_wait(0, 0)
+            low_gu.z_send(1, 0)
         elif tick == 5:
-            gu_y_forward(2)
-            gu_y_forward(3)
+            top_gu.z_wait(3)
+            top_gu.y_send(7)
+            low_gu.z_wait(0, 1)
+            low_gu.z_send(1, 1)
+            top_gu.y_forward(4)
+            dn.y_send(3)
         elif tick == 6:
-            dn_z_wait(1)
-            dn_z_send(2)
-            gu_y_forward(4)
+            dn.z_wait(2)
+            dn.z_send(3)
+            top_gu.y_forward(5)
+            top_gu.y_forward(6)
+            dn.y_send(4)
+            dn.y_forward(0)
+            low_gu.z_wait(1, 0)
+            low_gu.z_send(2, 0)
         elif tick == 7:
-            gu_y_forward(5)
+            low_gu.z_wait(1, 1)
+            low_gu.z_send(2, 1)
+            top_gu.y_forward(7)
+            dn.y_send(5)
+            dn.y_send(6)
+            dn.y_forward(1)
         elif tick == 8:
-            gu_y_forward(6)
+            low_gu.z_wait(2, 0)
+            low_gu.z_send(3, 0)
+            dn.z_wait(3)
+            dn.y_send(7)
+            dn.y_forward(2)
         elif tick == 9:
-            dn_z_wait(2)
-            dn_z_send(3)
-            gu_y_forward(7)
+            low_gu.z_wait(2, 1)
+            low_gu.z_send(3, 1)
+            dn.y_forward(3)
+            dn.y_forward(4)
+        elif tick == 10:
+            dn.y_forward(5)
+        elif tick == 11:
+            dn.y_forward(6)
+            dn.y_forward(7)
+            gu_wait()
+            up_block(0)
+        elif tick == 12:
+            up_block(1)
+
+    def gu_wait():
+        low_gu.taken(4, low_gu.along_z + 6)
+        top_gu.y_wait()
+
+    def dn_wait():
+        dn.y_wait()
 
     def run(stages, pump=None):
         for tick in range(CHUNKS + max(lag for lag, _ in stages)):
@@ -505,26 +569,15 @@
             if pump is not None:
                 pump(tick)
 
-    def first_of_block(stage):
-        def begin(i):
-            if i % PER_BLOCK == 0:
-                stage(i // PER_BLOCK)
-
-        return begin
-
     def join_first(i):
         swap_join(0, i)
 
     def relay_first(i):
         relay(0, i)
 
-    run(
-        (
-            (0, first_of_block(gated_block)), (1, join_first), (2, relay_first),
-            (3, stream_chunk), (4, spread_chunk), (5, far_chunk), (6, normed_chunk),
-        ),
-        pump,
-    )
+    def some_gated(i):
+        if i < BLOCKS:
+            gated_block(i)
 
     def silu(v):
         return v / (1.0 + jnp.exp(-v))
@@ -549,8 +602,8 @@
         hbuf[part, 640:768] = jnp.where(lane < 64, hidden, 0.0).astype(BF16)
 
     def down_block(g):
-        def term(b):
-            weights = dn_all[b * 4 : b * 4 + 4].reshape(256, dn_all.shape[2])
+        def term(j, core):
+            weights = dn_all[pl.ds((2 * j + core) * 4, 4)].reshape(256, dn_all.shape[2])
             return lax.dot_general(
                 hbuf[pl.ds(g * BLOCK, BLOCK)], weights, (((1,), (1,)), ((), ())),
                 preferred_element_type=F32,
@@ -565,13 +618,27 @@
         stores.append(pltpu.make_async_copy(out_ref.at[part], out_hbm.at[part], osem.at[i]))
         stores[-1].start()
 
-    def feed_block(g):
-        if g == 0:
-            gu_y_wait()
-        up_block(g)
-        if g == 0:
-            dn_z_wait(3)
-        down_block(g)
+    run(
+        (
+            (0, some_gated), (1, join_first), (2, relay_first),
+            (3, stream_chunk), (4, spread_chunk), (5, far_chunk), (6, normed_chunk),
+        ),
+        pump,
+    )
+
+    dn_wait()
+    down_block(0)
+    down_block(1)
+
+    def feed(tick):
+        if tick == 0:
+            up_block(2)
+        elif tick == 1:
+            down_block(2)
+        elif tick == 2:
+            up_block(3)
+        elif tick == 3:
+            down_block(3)
 
     def join_last(i):
         swap_join(1, i)
@@ -579,14 +646,15 @@
     def relay_last(i):
         relay(1, i)
 
-    run(((0, first_of_block(feed_block)), (1, join_last), (3, relay_last), (5, mixed_chunk)))
+    run(((0, join_last), (2, relay_last), (4, mixed_chunk)), feed)
 
     def drain():
         for copy in stores:
             copy.wait()
         for group in (*sums_out, gather_out):
             left(sbuf.at[pl.ds(0, 7)], group)
-        left(gu_all.at[pl.ds(0, 31)], gu_out)
+        left(gu_all.at[pl.ds(0, 31), pl.ds(0, gu_rows)], gu_out)
+        left(gu_all.at[pl.ds(0, 31), pl.ds(0, gu_rows)], low_out)
         left(dn_all.at[pl.ds(0, 31)], dn_out)
         left(s1_buf.at[pl.ds(0, NY - 1)], s1_out)
         left(s3_buf.at[pl.ds(0, NY - 1)], s3_out)
@@ -597,10 +665,10 @@
                 state_copy(d).wait_send()
 
     drain()
-    assert slots.used <= RECEIVES
-
-
-RECEIVES, SENDS = 144, 14
+    assert slots.used <= RECEIVES, slots.used
+
+
+RECEIVES, SENDS = 140, 15
 
 
 def local(

time: 104 us -> 95.8 us (0.921)
  Pallas kernels: 102 us -> 93.8 us
    pallas_call x1, Pallas kernels: 102 us -> 93.8 us  [local(): pl.pallas_call(cell_kernel, out_shape=jax.ShapeDtypeStruct(residual.shape...]
where the time goes in v3:
time: 95.8 us; the launch traced here: 95.7 us
  Pallas kernels  93.8 us (98%)
  local copies, waits for them, and re-layouts  1.87 us (2%)
    pallas_call x1, Pallas kernels, local(): pl.pallas_call(cell_kernel, out_shape=jax.ShapeDtypeStruct(residual.shape...  93.8 us

profile of v3, /device:TPU:1, one launch (start us, length us, event | category | flops | bytes accessed | tf_op | source)
XLA Modules:
  0.0 95.7 jit_solution(7568413394525164706)
XLA Ops:
  0.0 93.8 %shard_map.136 = bf16[1024,256]{1,0:T(8,128)(2,1)} custom-call(bf16[1024,128]{1,0:T(8,128)(2,1)} %q_in.1, bf16[1024,128]{1,0:T(8,128)(2,1)} %k_in.1, bf16[1024,256]{1,0:T(8,128)(2,1)} %v_in.1, bf16[1024,256]{1,0:T(8,128)(2,1)} %og_in.1, bf16[1,1024]{1,0:T(2,128)(2,1)} %ig_in.1, bf16[1,1024]{1,0:T(2,128)(2,1)} %fg_in.1, f32[1,1024]{1,0:T(1,128)} %ex_in.1, ...), custom_call_target="tpu_custom_call" | custom-call | tf_op jit(solution)/shard_map/pallas_call | solution.py:736
  93.8 1.9 %copy.16 = bf16[1024,256]{1,0:T(8,128)(2,1)} copy(bf16[1024,256]{1,0:T(8,128)(2,1)} %shard_map.136) | data formatting | bytes 1048576

commit v4 on v3

--- a/solution.py
+++ b/solution.py
@@ -16,7 +16,7 @@
 BLOCKS = 4
 PER_BLOCK = CHUNKS // BLOCKS
 BLOCK = 256
-EARLY = 2
+EARLY = ((0, 1), (0, 1, 2, 3, 4, 7))
 
 
 class Slots:
@@ -361,9 +361,10 @@
     top_gu.z_send(1)
     dn.z_send(0)
     top_gu.y_send(1)
+    top_gu.y_send(2)
     z_states()
     low_gu.y_forward()
-    top_gu.y_send(2)
+    top_gu.y_forward(0)
     dn.y_send(0)
     carried_top = carried()
 
@@ -385,7 +386,7 @@
         top, low = pl.ds(0, half), pl.ds(half, half)
         send(qbuf.at[a, i, x_at[2], top], rly.at[a, i, 0], n + 1, to_right, sums_out[a])
         send(qbuf.at[a, i, x_at[2], low], rly.at[a, i, 1], n + 2, to_left, sums_out[a])
-        if i < EARLY or (a == 1 and i == CHUNKS - 1):
+        if i in EARLY[a]:
             direct(a, i)
 
     def direct(a, i):
@@ -404,7 +405,7 @@
         added = rly[a, i, 1].astype(F32) + qbuf[a, i, x_at[3], half:].astype(F32)
         rsum[a, i, 1] = added.astype(BF16)
         send(rsum.at[a, i, 1], fin.at[a, i, 1, 1], n + 3, to_left, sums_out[a])
-        if i >= EARLY and not (a == 1 and i == CHUNKS - 1):
+        if i not in EARLY[a]:
             direct(a, i)
 
     def total(a, i):
@@ -491,68 +492,68 @@
             top_gu.y_send(4)
             dn.z_wait(0)
             dn.z_send(1)
+            dn.y_send(1)
         elif tick == 1:
             low_gu.z_send(0, 1)
         elif tick == 2:
-            top_gu.y_forward(0)
-            dn.y_send(1)
+            top_gu.y_forward(1)
+            dn.y_send(2)
         elif tick == 3:
             top_gu.z_wait(2)
             top_gu.z_send(3)
             top_gu.y_send(5)
             top_gu.y_send(6)
-            top_gu.y_forward(1)
+            top_gu.y_forward(2)
         elif tick == 4:
             dn.z_wait(1)
             dn.z_send(2)
-            dn.y_send(2)
-            top_gu.y_forward(2)
             top_gu.y_forward(3)
+            dn.y_send(3)
             low_gu.z_wait(0, 0)
             low_gu.z_send(1, 0)
         elif tick == 5:
             top_gu.z_wait(3)
             top_gu.y_send(7)
+            top_gu.y_forward(4)
+            dn.y_send(4)
             low_gu.z_wait(0, 1)
             low_gu.z_send(1, 1)
-            top_gu.y_forward(4)
-            dn.y_send(3)
         elif tick == 6:
             dn.z_wait(2)
             dn.z_send(3)
             top_gu.y_forward(5)
             top_gu.y_forward(6)
-            dn.y_send(4)
             dn.y_forward(0)
+            dn.y_send(5)
             low_gu.z_wait(1, 0)
             low_gu.z_send(2, 0)
         elif tick == 7:
+            top_gu.y_forward(7)
+            dn.y_send(6)
+            dn.y_forward(1)
+            dn.y_forward(2)
             low_gu.z_wait(1, 1)
             low_gu.z_send(2, 1)
-            top_gu.y_forward(7)
-            dn.y_send(5)
-            dn.y_send(6)
-            dn.y_forward(1)
         elif tick == 8:
+            dn.z_wait(3)
+            dn.y_send(7)
+            dn.y_forward(3)
             low_gu.z_wait(2, 0)
             low_gu.z_send(3, 0)
-            dn.z_wait(3)
-            dn.y_send(7)
-            dn.y_forward(2)
         elif tick == 9:
+            dn.y_forward(4)
+            dn.y_forward(5)
             low_gu.z_wait(2, 1)
             low_gu.z_send(3, 1)
-            dn.y_forward(3)
-            dn.y_forward(4)
         elif tick == 10:
-            dn.y_forward(5)
-        elif tick == 11:
             dn.y_forward(6)
             dn.y_forward(7)
+        elif tick == 11:
             gu_wait()
             up_block(0)
         elif tick == 12:
-            up_block(1)
+            dn_wait()
+            down_block(0)
 
     def gu_wait():
         low_gu.taken(4, low_gu.along_z + 6)
@@ -626,33 +627,9 @@
         pump,
     )
 
-    dn_wait()
-    down_block(0)
-    down_block(1)
-
-    def feed(tick):
-        if tick == 0:
-            up_block(2)
-        elif tick == 1:
-            down_block(2)
-        elif tick == 2:
-            up_block(3)
-        elif tick == 3:
-            down_block(3)
-
-    def join_last(i):
-        swap_join(1, i)
-
-    def relay_last(i):
-        relay(1, i)
-
-    run(((0, join_last), (2, relay_last), (4, mixed_chunk)), feed)
-
     def drain():
-        for copy in stores:
-            copy.wait()
-        for group in (*sums_out, gather_out):
-            left(sbuf.at[pl.ds(0, 7)], group)
+        left(sbuf.at[pl.ds(0, 7)], sums_out[0])
+        left(sbuf.at[pl.ds(0, 7)], gather_out)
         left(gu_all.at[pl.ds(0, 31), pl.ds(0, gu_rows)], gu_out)
         left(gu_all.at[pl.ds(0, 31), pl.ds(0, gu_rows)], low_out)
         left(dn_all.at[pl.ds(0, 31)], dn_out)
@@ -664,7 +641,31 @@
             def _(d=d):
                 state_copy(d).wait_send()
 
+    def last(*steps):
+        for name, at in steps:
+            if name == "up":
+                up_block(at)
+            elif name == "down":
+                down_block(at)
+            elif name == "join":
+                swap_join(1, at)
+            elif name == "relay":
+                relay(1, at)
+            else:
+                mixed_chunk(at)
+
+    last(
+        ("join", 0), ("up", 1), ("join", 1), ("down", 1), ("relay", 0), ("up", 2),
+        ("join", 2), ("relay", 1), ("down", 2), ("join", 3), ("up", 3), ("join", 4),
+        ("relay", 2), ("mixed", 0), ("down", 3), ("join", 5), ("relay", 3), ("mixed", 1),
+        ("join", 6), ("relay", 4), ("mixed", 2), ("join", 7), ("relay", 5), ("mixed", 3),
+        ("relay", 6), ("mixed", 4), ("relay", 7), ("mixed", 5), ("mixed", 6),
+    )
     drain()
+    mixed_chunk(7)
+    for copy in stores:
+        copy.wait()
+    left(sbuf.at[pl.ds(0, 7)], sums_out[1])
     assert slots.used <= RECEIVES, slots.used
 
 

time: 95.8 us -> 94.6 us (0.987)
  Pallas kernels: 93.8 us -> 92.6 us
    pallas_call x1, Pallas kernels: 93.8 us -> 92.6 us  [local(): pl.pallas_call(cell_kernel, out_shape=jax.ShapeDtypeStruct(residual.shape...]
where the time goes in v4:
time: 94.6 us; the launch traced here: 94.5 us
  Pallas kernels  92.6 us (98%)
  local copies, waits for them, and re-layouts  1.87 us (2%)
    pallas_call x1, Pallas kernels, local(): pl.pallas_call(cell_kernel, out_shape=jax.ShapeDtypeStruct(residual.shape...  92.6 us

profile of v4, /device:TPU:1, one launch (start us, length us, event | category | flops | bytes accessed | tf_op | source)
XLA Modules:
  0.0 94.5 jit_solution(207595850212276689)
XLA Ops:
  0.0 92.6 %shard_map.136 = bf16[1024,256]{1,0:T(8,128)(2,1)} custom-call(bf16[1024,128]{1,0:T(8,128)(2,1)} %q_in.1, bf16[1024,128]{1,0:T(8,128)(2,1)} %k_in.1, bf16[1024,256]{1,0:T(8,128)(2,1)} %v_in.1, bf16[1024,256]{1,0:T(8,128)(2,1)} %og_in.1, bf16[1,1024]{1,0:T(2,128)(2,1)} %ig_in.1, bf16[1,1024]{1,0:T(2,128)(2,1)} %fg_in.1, f32[1,1024]{1,0:T(1,128)} %ex_in.1, ...), custom_call_target="tpu_custom_call" | custom-call | tf_op jit(solution)/shard_map/pallas_call | solution.py:737
  92.6 1.9 %copy.16 = bf16[1024,256]{1,0:T(8,128)(2,1)} copy(bf16[1024,256]{1,0:T(8,128)(2,1)} %shard_map.136) | data formatting | bytes 1048576

commit v5 on v4

--- a/solution.py
+++ b/solution.py
@@ -543,14 +543,13 @@
         elif tick == 9:
             dn.y_forward(4)
             dn.y_forward(5)
-            low_gu.z_wait(2, 1)
-            low_gu.z_send(3, 1)
         elif tick == 10:
             dn.y_forward(6)
             dn.y_forward(7)
-        elif tick == 11:
             gu_wait()
             up_block(0)
+        elif tick == 11:
+            up_block(1)
         elif tick == 12:
             dn_wait()
             down_block(0)
@@ -567,6 +566,9 @@
             for lag, stage in stages:
                 if 0 <= tick - lag < CHUNKS:
                     stage(tick - lag)
+                if tick == 9 and lag == 3:
+                    low_gu.z_wait(2, 1)
+                    low_gu.z_send(3, 1)
             if pump is not None:
                 pump(tick)
 
@@ -655,11 +657,11 @@
                 mixed_chunk(at)
 
     last(
-        ("join", 0), ("up", 1), ("join", 1), ("down", 1), ("relay", 0), ("up", 2),
-        ("join", 2), ("relay", 1), ("down", 2), ("join", 3), ("up", 3), ("join", 4),
-        ("relay", 2), ("mixed", 0), ("down", 3), ("join", 5), ("relay", 3), ("mixed", 1),
-        ("join", 6), ("relay", 4), ("mixed", 2), ("join", 7), ("relay", 5), ("mixed", 3),
-        ("relay", 6), ("mixed", 4), ("relay", 7), ("mixed", 5), ("mixed", 6),
+        ("join", 0), ("down", 1), ("join", 1), ("up", 2), ("relay", 0), ("join", 2),
+        ("relay", 1), ("down", 2), ("join", 3), ("up", 3), ("relay", 2), ("join", 4),
+        ("mixed", 0), ("down", 3), ("join", 5), ("relay", 3), ("mixed", 1), ("join", 6),
+        ("relay", 4), ("mixed", 2), ("join", 7), ("relay", 5), ("mixed", 3), ("relay", 6),
+        ("mixed", 4), ("relay", 7), ("mixed", 5), ("mixed", 6),
     )
     drain()
     mixed_chunk(7)

time: 94.6 us -> 95 us (level)
  no operation moved by 1% of the time
where the time goes in v5:
time: 95 us; the launch traced here: 94.9 us
  Pallas kernels  93 us (98%)
  local copies, waits for them, and re-layouts  1.87 us (2%)
    pallas_call x1, Pallas kernels, local(): pl.pallas_call(cell_kernel, out_shape=jax.ShapeDtypeStruct(residual.shape...  93 us

profile of v5, /device:TPU:1, one launch (start us, length us, event | category | flops | bytes accessed | tf_op | source)
XLA Modules:
  0.0 94.9 jit_solution(6318600408579714721)
XLA Ops:
  0.0 93.0 %shard_map.136 = bf16[1024,256]{1,0:T(8,128)(2,1)} custom-call(bf16[1024,128]{1,0:T(8,128)(2,1)} %q_in.1, bf16[1024,128]{1,0:T(8,128)(2,1)} %k_in.1, bf16[1024,256]{1,0:T(8,128)(2,1)} %v_in.1, bf16[1024,256]{1,0:T(8,128)(2,1)} %og_in.1, bf16[1,1024]{1,0:T(2,128)(2,1)} %ig_in.1, bf16[1,1024]{1,0:T(2,128)(2,1)} %fg_in.1, f32[1,1024]{1,0:T(1,128)} %ex_in.1, ...), custom_call_target="tpu_custom_call" | custom-call | tf_op jit(solution)/shard_map/pallas_call | solution.py:739
  93.0 1.9 %copy.16 = bf16[1024,256]{1,0:T(8,128)(2,1)} copy(bf16[1024,256]{1,0:T(8,128)(2,1)} %shard_map.136) | data formatting | bytes 1048576
